TPU v7x, 256 devices: a whole 4x4x8 slice. The times are simulated.
256 devices in a mesh: sp: 32 (over z, x), tp: 8 (over y, core).
Axes of the slice: x: 4, y: 4, z: 8, core: 2. Of those that a mesh axis runs over, the one named last changes fastest.
Arguments:
- tokens: bfloat16 [32768, 2048], P('sp', 'tp'), may hold values from -70 to 70
- w_query: bfloat16 [2048, 1024], P(None, 'tp'), may hold values from -0.125 to 0.125
- w_key: bfloat16 [2048, 1024], P(None, 'tp'), may hold values from -0.125 to 0.125
- w_value: bfloat16 [2048, 1024], P(None, 'tp'), may hold values from -0.125 to 0.125
- w_delta_gate: bfloat16 [2048, 1024], P(None, 'tp'), may hold values from -0.125 to 0.125
- w_glu_value: bfloat16 [2048, 1024], P(None, 'tp'), may hold values from -0.125 to 0.125
- w_glu_gate: bfloat16 [2048, 1024], P(None, 'tp'), may hold values from -0.125 to 0.125
- w_conv_gate: bfloat16 [2048, 1024], P(None, 'tp'), may hold values from -0.125 to 0.125
- w_beta: bfloat16 [2048, 8], replicated, may hold values from -0.125 to 0.125
- w_decay: bfloat16 [2048, 8], replicated, may hold values from -0.125 to 0.125
- decay_log: float32 [8], replicated, may hold values from -12 to -3
- head_gain: float32 [128], replicated, may hold values from 0.1 to 1.9
- conv_taps: bfloat16 [31, 1024], P(None, 'tp'), may hold values from -2.5 to 2.5
- ln_gain: float32 [1024], P('tp'), may hold values from 0.1 to 1.9
- ln_shift: float32 [1024], P('tp'), may hold values from -3 to 3
- out_delta: bfloat16 [1024, 2048], P('tp'), may hold values from -0.125 to 0.125
- out_conv: bfloat16 [1024, 2048], P('tp'), may hold values from -0.125 to 0.125
Outputs:
- mixed_out: bfloat16 [32768, 2048], P(('sp', 'tp'))
All inputs are finite; a program needn't handle non-finite values.
Results may differ from a plain program's by a relative error of at most 0.024.
Values may be sent and summed in bfloat16 or wider, within the bound.
A program may use at most 64 MiB of HBM per device.

v0:
```python
import functools

import jax
import jax.numpy as jnp
from jax import lax
from jax.experimental import pallas as pl
from jax.experimental.pallas import tpu as pltpu
from jax.sharding import PartitionSpec as P

BLOCK = 128
CHUNKS = 8
TOGETHER = 8
CUTS = 8


TINY_NORM = 1e-06
TINY_VAR = 1e-05
HIGHEST = lax.Precision.HIGHEST


def nt(a, b):
    return lax.dot_general(a, b, (((1,), (1,)), ((), ())), preferred_element_type=jnp.float32)


def mm(a, b):
    return jnp.dot(
        a.astype(jnp.bfloat16), b.astype(jnp.bfloat16), preferred_element_type=jnp.float32
    )


def delta_kernel(
    heads, width, q_ref, k_ref, v_ref, g_ref, outa_ref, outb_ref, final_ref,
    lhs_s, corr_s, score_s, wt_s, tail_s, state_ref,
):
    rows = q_ref.shape[0]
    blocks = rows // BLOCK
    row_id = lax.broadcasted_iota(jnp.int32, (BLOCK, BLOCK), 0)
    col_id = lax.broadcasted_iota(jnp.int32, (BLOCK, BLOCK), 1)
    causal = row_id >= col_id
    strict = row_id > col_id
    differ = row_id ^ col_id
    eye = jnp.where(row_id == col_id, 1.0, 0.0)
    tril = jnp.where(causal, 1.0, 0.0)

    def prepare(c):
        at = pl.ds(pl.multiple_of(c * BLOCK, BLOCK), BLOCK)
        gates = g_ref[at, :]
        sums = jnp.dot(tril, gates, precision=HIGHEST, preferred_element_type=jnp.float32)
        chains = []
        for h in range(heads):
            lanes = slice(h * width, (h + 1) * width)
            k, q = k_ref[at, lanes], q_ref[at, lanes]
            v = v_ref[at, lanes].astype(jnp.float32)
            kf, qf = k.astype(jnp.float32), q.astype(jnp.float32)
            ik = lax.rsqrt(jnp.sum(kf * kf, axis=-1, keepdims=True) + TINY_NORM)
            iq = lax.rsqrt(jnp.sum(qf * qf, axis=-1, keepdims=True) + TINY_NORM)
            iq = iq * width ** (-0.5)
            beta = gates[:, h : h + 1]
            log_sum = sums[:, heads + h : heads + h + 1]
            log_full = jnp.broadcast_to(log_sum, (BLOCK, BLOCK))
            spread = log_full - log_full.T
            damp = jnp.where(causal, jnp.exp(jnp.where(causal, spread, 0.0)), 0.0)
            damp = damp * jnp.broadcast_to(ik, (BLOCK, BLOCK)).T
            lower = jnp.where(strict, nt(k, k) * damp * (beta * ik), 0.0)
            score_s[h, at, :] = (nt(q, k) * damp * iq).astype(jnp.bfloat16)
            grow = jnp.exp(log_sum)
            right = jnp.concatenate([v * beta, kf * (beta * ik * grow)], axis=1)
            tail = log_full[BLOCK - 1 : BLOCK, :]
            weighted = kf * (ik * jnp.exp(tail[:, :1] - log_sum))
            wt_s[h, c] = weighted.T.astype(jnp.bfloat16)
            tail_s[h, c] = jnp.broadcast_to(jnp.exp(tail), (8, BLOCK))
            lhs_s[h, c, BLOCK:, :] = (qf * (iq * grow)).astype(jnp.bfloat16)
            chains.append([h, lower, right, eye - jnp.where(differ == 1, lower, 0.0)])
        return at, c, chains

    def pair(p, carry):
        prepared = [prepare(p * TOGETHER + i) for i in range(TOGETHER)]
        size = 2
        while size < BLOCK:
            level = (differ >= size) & (differ < 2 * size)
            parts = [
                [mm(jnp.where(level, ch[1], 0.0), ch[3]) for ch in item[2]] for item in prepared
            ]
            for item, part in zip(prepared, parts):
                for ch, moved in zip(item[2], part):
                    ch[3] = ch[3] - mm(ch[3], moved)
            size *= 2
        for at, c, chains in prepared:
            for h, lower, right, inverse in chains:
                solved = mm(inverse, right)
                corr_s[h, at, :] = solved[:, :width]
                lhs_s[h, c, :BLOCK, :] = solved[:, width:].astype(jnp.bfloat16)
        return carry

    lax.fori_loop(0, blocks // TOGETHER, pair, 0)
    for h in range(heads):
        state_ref[h] = jnp.concatenate([eye, jnp.zeros((width, width), jnp.float32)], axis=1)

    def advance(c, carry):
        at = pl.ds(pl.multiple_of(c * BLOCK, BLOCK), BLOCK)
        boths = [mm(lhs_s[h, c], state_ref[h]) for h in range(heads)]
        fresh = []
        for h in range(heads):
            first = boths[h][:BLOCK]
            fresh.append(
                jnp.concatenate(
                    [-first[:, :width], corr_s[h, at, :] - first[:, width:]], axis=1
                ).astype(jnp.bfloat16)
            )
        for h in range(heads):
            decay = tail_s[h, c][:1, :]
            decay = jnp.concatenate([decay, decay], axis=1)
            state_ref[h] = state_ref[h] * decay + mm(wt_s[h, c], fresh[h])
        for h in range(heads):
            out = boths[h][BLOCK:] + mm(score_s[h, at, :], fresh[h])
            outa_ref[h, at, :] = out[:, :width].astype(jnp.bfloat16)
            outb_ref[h, at, :] = out[:, width:]
        return carry

    lax.fori_loop(0, blocks, advance, 0)
    final_ref[...] = state_ref[...].astype(jnp.bfloat16)


def delta_rule(query_raw, key_raw, value_raw, gates, heads, width):
    rows = query_raw.shape[0]
    blocks = rows // BLOCK
    vm = pl.BlockSpec(memory_space=pltpu.VMEM)
    return pl.pallas_call(
        functools.partial(delta_kernel, heads, width),
        out_shape=(
            jax.ShapeDtypeStruct((heads, rows, width), jnp.bfloat16),
            jax.ShapeDtypeStruct((heads, rows, width), jnp.float32),
            jax.ShapeDtypeStruct((heads, width, 2 * width), jnp.bfloat16),
        ),
        in_specs=[vm] * 4,
        out_specs=(vm, vm, vm),
        scratch_shapes=[
            pltpu.VMEM((heads, blocks, 2 * BLOCK, width), jnp.bfloat16),
            pltpu.VMEM((heads, rows, width), jnp.float32),
            pltpu.VMEM((heads, rows, BLOCK), jnp.bfloat16),
            pltpu.VMEM((heads, blocks, width, BLOCK), jnp.bfloat16),
            pltpu.VMEM((heads, blocks, 8, BLOCK), jnp.float32),
            pltpu.VMEM((heads, width, 2 * width), jnp.float32),
        ],
        compiler_params=pltpu.CompilerParams(
            vmem_limit_bytes=40 * 1024 * 1024
        ),
        cost_estimate=pl.CostEstimate(
            flops=10_000_000_000, bytes_accessed=4_000_000, transcendentals=0
        ),
        name="delta_rule",
    )(query_raw, key_raw, value_raw, gates)


MESH = pl.DeviceIdType.MESH


def sharded_place():
    tp = lax.axis_size("tp")
    me = lax.axis_index("tp")
    core = lax.rem(me, 2)
    return tp // 2, me, core, me // 2, me + 1 - 2 * core


def greet(chips, core, chip, sibling):
    barrier = pltpu.get_barrier_semaphore()
    pl.semaphore_signal(barrier, inc=1, device_id={"tp": sibling}, device_id_type=MESH)
    for o in range(1, chips):
        there = lax.rem(chip + o, chips) * 2 + core
        pl.semaphore_signal(barrier, inc=1, device_id={"tp": there}, device_id_type=MESH)
    pl.semaphore_wait(barrier, chips)


def project_kernel(heads, *refs):
    count = 7
    tok_ref, far_refs, wg_ref, rate_ref = refs[0], refs[1 : 1 + count], refs[8], refs[9]
    out_refs, gates_ref = refs[10 : 10 + count], refs[17]
    full, y_send, y_recv, own_send, own_recv, fwd_send, fwd_recv, w_sem = refs[18:26]
    w_refs = refs[26:]
    rows, part = tok_ref.shape
    step = rows // CHUNKS
    chips, me, core, chip, sibling = sharded_place()

    def columns(owner):
        return pl.ds(pl.multiple_of(owner * part, part), part)

    def at(r):
        return pl.ds(pl.multiple_of(r * step, step), step)

    def across(o, r):
        there = lax.rem(chip + o, chips) * 2 + core
        return pltpu.make_async_remote_copy(
            src_ref=tok_ref.at[at(r), :],
            dst_ref=full.at[at(r), columns(me)],
            send_sem=y_send.at[o - 1, r],
            recv_sem=y_recv.at[o - 1, r],
            device_id={"tp": there},
            device_id_type=MESH,
        )

    def beside(r):
        return pltpu.make_async_remote_copy(
            src_ref=tok_ref.at[at(r), :],
            dst_ref=full.at[at(r), columns(me)],
            send_sem=own_send.at[r],
            recv_sem=own_recv.at[r],
            device_id={"tp": sibling},
            device_id_type=MESH,
        )

    def forward(o, r):
        owner = lax.rem(chip - o + chips, chips) * 2 + core
        block = full.at[at(r), columns(owner)]
        return pltpu.make_async_remote_copy(
            src_ref=block,
            dst_ref=block,
            send_sem=fwd_send.at[o - 1, r],
            recv_sem=fwd_recv.at[o - 1, r],
            device_id={"tp": sibling},
            device_id_type=MESH,
        )

    greet(chips, core, chip, sibling)
    for r in range(CHUNKS):
        for o in range(1, chips):
            across(o, r).start()
    loads = [
        pltpu.make_async_copy(far, w_ref, w_sem.at[i])
        for i, (far, w_ref) in enumerate(zip(far_refs, w_refs))
    ]
    for load in loads:
        load.start()
    for r in range(CHUNKS):
        beside(r).start()
    full[:, columns(me)] = tok_ref[...]

    def chunk(first, pieces, carry):
        for i in range(pieces):
            for o in range(1, chips):
                across(o, first + i).wait_recv()
                forward(o, first + i).start()
        for i in range(pieces):
            beside(first + i).wait_recv()
            for o in range(1, chips):
                forward(o, first + i).wait_recv()
        size = step * pieces
        here = pl.ds(pl.multiple_of(first * step, step), size)
        squares = jnp.zeros((size, 1), jnp.float32)
        for b in range(2 * chips):
            piece = full[here, b * part : (b + 1) * part].astype(jnp.float32)
            squares = squares + jnp.sum(piece * piece, axis=1, keepdims=True)
        inv_rms = lax.rsqrt(squares / (part * 2 * chips) + TINY_NORM)
        for w_ref, out_ref in zip(w_refs, out_refs):
            summed = jnp.dot(full[here, :], w_ref[...], preferred_element_type=jnp.float32)
            out_ref[here, :] = (summed * inv_rms).astype(jnp.bfloat16)
        raw = jnp.dot(full[here, :], wg_ref[...], preferred_element_type=jnp.float32) * inv_rms
        lane = lax.broadcasted_iota(jnp.int32, raw.shape, 1)
        softplus = jnp.maximum(raw, 0.0) + jnp.log1p(jnp.exp(-jnp.abs(raw)))
        gates_ref[here, :] = jnp.where(lane < heads, jax.nn.sigmoid(raw), -rate_ref[...] * softplus)
        return carry

    for load in loads:
        load.wait()
    paired = CHUNKS // 2 - 1
    lax.fori_loop(0, paired, lambda r, carry: chunk(2 * r, 2, carry), 0)
    lax.fori_loop(2 * paired, CHUNKS, lambda r, carry: chunk(r, 1, carry), 0)
    for r in range(CHUNKS):
        for o in range(1, chips):
            across(o, r).wait_send()
            forward(o, r).wait_send()
        beside(r).wait_send()


def project(tokens, weights, w_gates, rates, heads):
    rows, part = tokens.shape
    tp = lax.axis_size("tp")
    others = max(tp // 2 - 1, 1)
    vm = pl.BlockSpec(memory_space=pltpu.VMEM)
    dma = pltpu.SemaphoreType.DMA
    return pl.pallas_call(
        functools.partial(project_kernel, heads),
        out_shape=tuple(
            jax.ShapeDtypeStruct((rows, w.shape[1]), jnp.bfloat16) for w in weights
        )
        + (jax.ShapeDtypeStruct((rows, w_gates.shape[1]), jnp.float32),),
        in_specs=[vm] + [pl.BlockSpec(memory_space=pl.ANY)] * len(weights) + [vm] * 2,
        out_specs=(vm,) * (1 + len(weights)),
        scratch_shapes=[
            pltpu.VMEM((rows, part * tp), jnp.bfloat16),
            dma((others, CHUNKS)),
            dma((others, CHUNKS)),
            dma((CHUNKS,)),
            dma((CHUNKS,)),
            dma((others, CHUNKS)),
            dma((others, CHUNKS)),
            dma((len(weights),)),
        ]
        + [pltpu.VMEM(w.shape, w.dtype) for w in weights],
        compiler_params=pltpu.CompilerParams(
            collective_id=0, has_side_effects=True, vmem_limit_bytes=48 * 1024 * 1024
        ),
        cost_estimate=pl.CostEstimate(
            flops=10_000_000_000, bytes_accessed=20_000_000, transcendentals=0
        ),
        name="gather_project",
    )(tokens, *weights, w_gates, rates)


def middle_kernel(
    heads, width, final_ref, gv_ref, gg_ref, cg_ref, taps_ref, ln_gain_ref, ln_shift_ref,
    outa_ref, outb_ref, dg_ref, gain_ref, mixed_ref, conv_ref,
    padded, filtered, halo_out, halo_in, sums_out, sums_in, near, window_s, sent_s, far_s,
    near_send, near_recv, far_send, far_recv, halo_send, halo_recv, ln_send, ln_recv,
):
    rows = gv_ref.shape[0]
    halo = halo_in.shape[0]
    lanes = padded.shape[2]
    groups = padded.shape[0]
    kernel = taps_ref.shape[0]
    tiles = rows // BLOCK
    sp, place = lax.axis_size("sp"), lax.axis_index("sp")
    tp, me = lax.axis_size("tp"), lax.axis_index("tp")
    reaches = [2]
    while 2 * reaches[-1] < sp:
        reaches.append(2 * reaches[-1])
    distances = [1, 2] + reaches[1:]
    barrier = pltpu.get_barrier_semaphore()
    for step in distances:
        for to in (step, sp - step):
            pl.semaphore_signal(
                barrier, inc=1, device_id={"sp": lax.rem(place + to, sp)}, device_id_type=MESH
            )
    for step in range(1, tp):
        pl.semaphore_signal(
            barrier, inc=1, device_id={"tp": lax.rem(me + step, tp)}, device_id_type=MESH
        )
    pl.semaphore_wait(barrier, 2 * len(distances) + tp - 1)

    def onward(src, dst, send, recv, step):
        return pltpu.make_async_remote_copy(
            src_ref=src,
            dst_ref=dst,
            send_sem=send,
            recv_sem=recv,
            device_id={"sp": lax.rem(place + step, sp)},
            device_id_type=MESH,
        )

    firsts = [
        onward(final_ref, near.at[i], near_send.at[i], near_recv.at[i], i + 1) for i in range(2)
    ]
    for copy in firsts:
        copy.start()

    def at(t):
        return pl.ds(pl.multiple_of(t * BLOCK, BLOCK), BLOCK)

    def unit(t, carry):
        value = gv_ref[at(t), :].astype(jnp.float32)
        units = (value * jax.nn.sigmoid(gg_ref[at(t), :].astype(jnp.float32))).astype(jnp.bfloat16)
        wide = units.astype(jnp.float32)
        for g in range(groups):
            padded[g, pl.ds(pl.multiple_of(t * BLOCK + halo, halo), BLOCK), :] = wide[
                :, g * lanes : (g + 1) * lanes
            ]
        return units

    units = unit(tiles - 1, 0)
    halo_out[...] = units[BLOCK - halo :, :]
    halo_copy = onward(halo_out, halo_in, halo_send.at[0], halo_recv.at[0], 1)
    halo_copy.start()

    def unit_loop(t, carry):
        unit(t, 0)
        return carry

    lax.fori_loop(0, tiles - 1, unit_loop, 0)

    def conv(t, carry):
        first = jnp.zeros((BLOCK, 1), jnp.float32)
        second = jnp.zeros((BLOCK, 1), jnp.float32)
        for g in range(groups):
            total = jnp.zeros((BLOCK, lanes), jnp.float32)
            for j in range(kernel):
                start = t * BLOCK + (halo - kernel + 1 + j)
                tap = taps_ref[j : j + 1, g * lanes : (g + 1) * lanes]
                total = total + padded[g, pl.ds(start, BLOCK), :] * tap
            filtered[g, at(t), :] = total
            first = first + jnp.sum(total, axis=1, keepdims=True)
            second = second + jnp.sum(total * total, axis=1, keepdims=True)
        lane = lax.broadcasted_iota(jnp.int32, (BLOCK, BLOCK), 1)
        sums_out[t] = jnp.where(lane == 0, first, jnp.where(lane == 1, second, 0.0)).T[:8, :]
        return carry

    half = tiles // 2
    lax.fori_loop(1, half, conv, 0)
    for copy in firsts:
        copy.wait()
    for h in range(heads):
        one = jnp.where(place >= 1, near[0, h].astype(jnp.float32), 0.0)
        two = jnp.where(place >= 2, near[1, h].astype(jnp.float32), 0.0)
        moved = mm(one[:, :width], two)
        window_s[h] = jnp.concatenate(
            [moved[:, :width], moved[:, width:] + one[:, width:]], axis=1
        )
        sent_s[0, h] = window_s[h].astype(jnp.bfloat16)

    def step_copy(i):
        return onward(sent_s.at[i], far_s.at[i], far_send.at[i], far_recv.at[i], reaches[i])

    step_copy(0).start()
    lax.fori_loop(half, tiles, conv, 0)
    halo_copy.wait()
    before = jnp.where(place >= 1, halo_in[...].astype(jnp.float32), 0.0)
    for g in range(groups):
        padded[g, :halo, :] = before[:, g * lanes : (g + 1) * lanes]
    conv(0, 0)

    def ln_copy(step):
        return pltpu.make_async_remote_copy(
            src_ref=sums_out,
            dst_ref=sums_in.at[step - 1],
            send_sem=ln_send.at[step - 1],
            recv_sem=ln_recv.at[step - 1],
            device_id={"tp": lax.rem(me + step, tp)},
            device_id_type=MESH,
        )

    for step in range(1, tp):
        ln_copy(step).start()
    for i in range(len(reaches) - 1):
        step_copy(i).wait()
        for h in range(heads):
            earlier = jnp.where(place >= reaches[i], far_s[i, h].astype(jnp.float32), 0.0)
            window = window_s[h]
            moved = mm(window[:, :width], earlier)
            window_s[h] = jnp.concatenate(
                [moved[:, :width], moved[:, width:] + window[:, width:]], axis=1
            )
            sent_s[i + 1, h] = window_s[h].astype(jnp.bfloat16)
        step_copy(i + 1).start()
    for step in range(1, tp):
        ln_copy(step).wait()
    channels = groups * lanes * tp

    def norm(t, carry):
        sums = sums_out[t]
        for step in range(1, tp):
            sums = sums + sums_in[step - 1, t]
        sums = jnp.concatenate([sums, jnp.zeros((BLOCK - 8, BLOCK), jnp.float32)], axis=0).T
        center = sums[:, 0:1] / channels
        variance = jnp.maximum(sums[:, 1:2] / channels - center * center, 0.0)
        scale = lax.rsqrt(variance + TINY_VAR)
        for g in range(groups):
            cut = slice(g * lanes, (g + 1) * lanes)
            normed = (filtered[g, at(t), :] - center) * scale
            normed = normed * ln_gain_ref[:, cut] + ln_shift_ref[:, cut]
            gate = cg_ref[at(t), cut].astype(jnp.float32)
            conv_ref[at(t), cut] = (jax.nn.silu(normed) * jax.nn.silu(gate)).astype(jnp.bfloat16)
        return carry

    lax.fori_loop(0, tiles, norm, 0)
    last = len(reaches) - 1
    step_copy(last).wait()
    carried = []
    for h in range(heads):
        earlier = jnp.where(
            place >= reaches[last], far_s[last, h, :, width:].astype(jnp.float32), 0.0
        )
        window = window_s[h]
        carried.append((mm(window[:, :width], earlier) + window[:, width:]).astype(jnp.bfloat16))

    def one_tile(t, carry):
        for h in range(heads):
            cut = slice(h * width, (h + 1) * width)
            result = outb_ref[h, at(t), :] + mm(outa_ref[h, at(t), :], carried[h])
            result = result * lax.rsqrt(
                jnp.mean(result * result, axis=-1, keepdims=True) + TINY_NORM
            )
            gate = dg_ref[at(t), cut].astype(jnp.float32)
            mixed_ref[at(t), cut] = (result * gain_ref[...] * jax.nn.silu(gate)).astype(
                jnp.bfloat16
            )
        return carry

    lax.fori_loop(0, tiles, one_tile, 0)


def middle(final, glu_value, glu_gate, conv_gate, taps, ln_gain, ln_shift, outa, outb, gate, gain):
    heads, width = final.shape[0], final.shape[1]
    rows, channels = glu_value.shape
    kernel = taps.shape[0]
    halo = (kernel - 1 + 31) // 32 * 32
    lanes = min(channels, 128)
    groups = channels // lanes
    sp, tp = lax.axis_size("sp"), lax.axis_size("tp")
    steps = 1
    while 2 ** (steps + 1) < sp:
        steps += 1
    vm = pl.BlockSpec(memory_space=pltpu.VMEM)
    dma = pltpu.SemaphoreType.DMA
    tiles = rows // BLOCK
    pair = (heads, width, 2 * width)
    return pl.pallas_call(
        functools.partial(middle_kernel, heads, width),
        out_shape=(
            jax.ShapeDtypeStruct((rows, heads * width), jnp.bfloat16),
            jax.ShapeDtypeStruct((rows, channels), jnp.bfloat16),
        ),
        in_specs=[vm] * 11,
        out_specs=(vm, vm),
        scratch_shapes=[
            pltpu.VMEM((groups, halo + rows, lanes), jnp.float32),
            pltpu.VMEM((groups, rows, lanes), jnp.float32),
            pltpu.VMEM((halo, channels), jnp.bfloat16),
            pltpu.VMEM((halo, channels), jnp.bfloat16),
            pltpu.VMEM((tiles, 8, BLOCK), jnp.float32),
            pltpu.VMEM((tp - 1, tiles, 8, BLOCK), jnp.float32),
            pltpu.VMEM((2,) + pair, jnp.bfloat16),
            pltpu.VMEM(pair, jnp.float32),
            pltpu.VMEM((steps,) + pair, jnp.bfloat16),
            pltpu.VMEM((steps,) + pair, jnp.bfloat16),
            dma((2,)),
            dma((2,)),
            dma((steps,)),
            dma((steps,)),
            dma((1,)),
            dma((1,)),
            dma((tp - 1,)),
            dma((tp - 1,)),
        ],
        compiler_params=pltpu.CompilerParams(
            collective_id=2, has_side_effects=True, vmem_limit_bytes=40 * 1024 * 1024
        ),
        cost_estimate=pl.CostEstimate(
            flops=10_000_000_000, bytes_accessed=20_000_000, transcendentals=0
        ),
        name="exchange_middle",
    )(final, glu_value, glu_gate, conv_gate, taps, ln_gain, ln_shift, outa, outb, gate, gain)


def output_kernel(
    dm_ref, cm_ref, wd_ref, wc_ref, out_ref,
    beside_out, beside_in, across_out, across_in, b_send, b_recv, y_send, y_recv,
):
    chips, me, core, chip, sibling = sharded_place()
    rows = out_ref.shape[0]
    width = out_ref.shape[1] // CUTS

    def cols(n):
        return pl.ds(pl.multiple_of(n * width, width), width)

    def partial(target, n):
        at = pl.ds(pl.multiple_of(target * rows, rows), rows)
        summed = jnp.dot(dm_ref[at, :], wd_ref[:, cols(n)], preferred_element_type=jnp.float32)
        return summed + jnp.dot(
            cm_ref[at, :], wc_ref[:, cols(n)], preferred_element_type=jnp.float32
        )

    def beside(o, n):
        return pltpu.make_async_remote_copy(
            src_ref=beside_out.at[o, n],
            dst_ref=beside_in.at[o, n],
            send_sem=b_send.at[o, n],
            recv_sem=b_recv.at[o, n],
            device_id={"tp": sibling},
            device_id_type=MESH,
        )

    def across(o, n):
        there = lax.rem(chip + o, chips) * 2 + core
        return pltpu.make_async_remote_copy(
            src_ref=across_out.at[o - 1, n],
            dst_ref=across_in.at[o - 1, n],
            send_sem=y_send.at[o - 1, n],
            recv_sem=y_recv.at[o - 1, n],
            device_id={"tp": there},
            device_id_type=MESH,
        )

    greet(chips, core, chip, sibling)
    order = list(range(1, chips)) + [0]
    for o in order:
        their_chip = lax.rem(chip + o, chips) * 2

        def give(n, carry, o=o, their_chip=their_chip):
            beside_out[o, n] = partial(their_chip + 1 - core, n).astype(jnp.bfloat16)
            beside(o, n).start()
            return carry

        def keep(n, carry, o=o, their_chip=their_chip):
            mine = partial(their_chip + core, n)
            beside(o, n).wait_recv()
            mine = mine + beside_in[o, n].astype(jnp.float32)
            across_out[o - 1, n] = mine.astype(jnp.bfloat16)
            across(o, n).start()
            return carry

        if o != 0:

            def both(n, carry, give=give, keep=keep):
                @pl.when(n + 1 < CUTS)
                def _():
                    give(n + 1, 0)

                return keep(n, carry)

            give(0, 0)
            lax.fori_loop(0, CUTS, both, 0)
        else:
            lax.fori_loop(0, CUTS, give, 0)

    def close(n, carry):
        mine = partial(me, n)
        beside(0, n).wait_recv()
        mine = mine + beside_in[0, n].astype(jnp.float32)
        for o in range(1, chips):
            across(o, n).wait_recv()
            mine = mine + across_in[o - 1, n].astype(jnp.float32)
        out_ref[:, cols(n)] = mine.astype(jnp.bfloat16)
        return carry

    lax.fori_loop(0, CUTS, close, 0)

    def drain(n, carry):
        for o in range(chips):
            beside(o, n).wait_send()
        for o in range(1, chips):
            across(o, n).wait_send()
        return carry

    lax.fori_loop(0, CUTS, drain, 0)


def output_projection(delta_mixed, conv_mixed, out_delta, out_conv):
    tp = lax.axis_size("tp")
    chips = tp // 2
    others = max(chips - 1, 1)
    rows = delta_mixed.shape[0] // tp
    width = out_delta.shape[1]
    cut = width // CUTS
    vm = pl.BlockSpec(memory_space=pltpu.VMEM)
    dma = pltpu.SemaphoreType.DMA
    return pl.pallas_call(
        output_kernel,
        out_shape=jax.ShapeDtypeStruct((rows, width), jnp.bfloat16),
        in_specs=[vm] * 4,
        out_specs=vm,
        scratch_shapes=[
            pltpu.VMEM((chips, CUTS, rows, cut), jnp.bfloat16),
            pltpu.VMEM((chips, CUTS, rows, cut), jnp.bfloat16),
            pltpu.VMEM((others, CUTS, rows, cut), jnp.bfloat16),
            pltpu.VMEM((others, CUTS, rows, cut), jnp.bfloat16),
            dma((chips, CUTS)),
            dma((chips, CUTS)),
            dma((others, CUTS)),
            dma((others, CUTS)),
        ],
        compiler_params=pltpu.CompilerParams(
            collective_id=1, has_side_effects=True, vmem_limit_bytes=48 * 1024 * 1024
        ),
        cost_estimate=pl.CostEstimate(
            flops=10_000_000_000, bytes_accessed=20_000_000, transcendentals=0
        ),
        name="output_scatter",
    )(delta_mixed, conv_mixed, out_delta, out_conv)


def local(
    tokens,
    w_query,
    w_key,
    w_value,
    w_delta_gate,
    w_glu_value,
    w_glu_gate,
    w_conv_gate,
    w_beta,
    w_decay,
    decay_log,
    head_gain,
    conv_taps,
    ln_gain,
    ln_shift,
    out_delta,
    out_conv,
):
    head_size = head_gain.shape[0]
    heads_here = w_query.shape[1] // head_size
    first_head = lax.axis_index("tp") * heads_here
    rates = jnp.exp(lax.dynamic_slice_in_dim(decay_log, first_head, heads_here, 0))
    fill = head_size - 2 * heads_here
    rates = jnp.concatenate(
        [jnp.zeros((heads_here,), jnp.float32), rates, jnp.zeros((fill,), jnp.float32)]
    )[None, :]
    w_gates = jnp.concatenate(
        [
            lax.dynamic_slice_in_dim(w_beta, first_head, heads_here, 1),
            lax.dynamic_slice_in_dim(w_decay, first_head, heads_here, 1),
            jnp.zeros((w_beta.shape[0], fill), jnp.bfloat16),
        ],
        axis=1,
    )
    weights = (w_query, w_key, w_value, w_delta_gate, w_glu_value, w_glu_gate, w_conv_gate)
    (
        query_raw,
        key_raw,
        value_raw,
        delta_gate_raw,
        glu_value_raw,
        glu_gate_raw,
        conv_gate_raw,
        gates,
    ) = project(tokens, weights, w_gates, rates, heads_here)
    outa, outb, final = delta_rule(
        query_raw, key_raw, value_raw, gates, heads_here, head_size
    )
    delta_mixed, conv_mixed = middle(
        final,
        glu_value_raw,
        glu_gate_raw,
        conv_gate_raw,
        conv_taps.astype(jnp.float32),
        ln_gain[None, :],
        ln_shift[None, :],
        outa,
        outb,
        delta_gate_raw,
        head_gain[None, :],
    )
    return output_projection(delta_mixed, conv_mixed, out_delta, out_conv)


def solution(mesh):
    return jax.shard_map(
        local,
        mesh=mesh,
        in_specs=(
            P("sp", "tp"),
            P(None, "tp"),
            P(None, "tp"),
            P(None, "tp"),
            P(None, "tp"),
            P(None, "tp"),
            P(None, "tp"),
            P(None, "tp"),
            P(),
            P(),
            P(),
            P(),
            P(None, "tp"),
            P("tp"),
            P("tp"),
            P("tp", None),
            P("tp", None),
        ),
        out_specs=P(("sp", "tp"), None),
        check_vma=False,
    )
```

profile of v0, /device:TPU:1, one launch (start us, length us, event | category | flops | bytes accessed | tf_op | source)
XLA Modules:
  0.0 118.4 jit_solution(3934624887398606332)
XLA Ops:
  0.0 0.8 constant_dynamic-slice_fusion
  0.8 0.0 copy-start.4
  0.8 0.3 copy.20
  1.1 0.0 copy-start.3
  1.1 0.3 copy.21
  1.5 0.1 pad.5.clone
  1.5 0.0 copy-start.13
  1.5 0.0 copy-start
  1.5 0.0 copy-start.1
  1.5 0.0 copy-start.2
  1.6 1.1 maximum_maximum_fusion.refs_8_
  2.7 0.0 copy-done.13
  2.7 0.6 dynamic_slice.11
  3.8 0.1 maximum_bitcast_fusion.refs_9_
  3.9 0.0 copy-done.4
  3.9 0.0 copy-done.3
  3.9 0.0 copy-done
  3.9 0.0 copy-done.1
  3.9 0.0 copy-done.2
  3.9 0.0 copy-start.5
  3.9 1.0 copy-done.5
  5.0 0.0 copy-start.6
  5.0 1.0 copy-done.6
  6.0 35.5 %gather_project.1 = (bf16[1024,128]{1,0:T(8,128)(2,1)S(1)}, bf16[1024,128]{1,0:T(8,128)(2,1)S(1)}, bf16[1024,128]{1,0:T(8,128)(2,1)S(1)}, bf16[1024,128]{1,0:T(8...) custom-call(bf16[1024,256]{1,0:T(8,128)(2,1)S(1)} %copy-done, ...), custom_call_target="tpu_custom_call" | custom-call | flops 10000000000 | bytes 20000000 | tf_op jit(solution)/shard_map/gather_project/pallas_call | solution.py:280
  41.5 6.4 %delta_rule.1 = (bf16[1,1024,128]{2,1,0:T(8,128)(2,1)S(1)}, f32[1,1024,128]{2,1,0:T(8,128)S(1)}, bf16[1,128,256]{2,1,0:T(8,128)(2,1)S(1)}) custom-call(bf16[1024,128]{1,0:T(8,128)(2,1)S(1)} %get-tuple-element.18.q_ref, bf16[1024,128]{1,0:T(8,128)(2,1)S(1)} %get-tuple-element.19.k_ref, bf16[1024,128]{1,0:T(8,128)(2,1)S(1)} %get-tuple-element.20.v_ref, ...), custom_call_target="tpu_custom_call" | custom-call | flops 10000000000 | bytes 4000000 | tf_op jit(solution)/shard_map/delta_rule/pallas_call | solution.py:128
  48.0 0.0 copy-start.12
  48.0 0.7 copy-done.12
  48.7 0.0 copy-start.9
  48.7 0.0 copy-start.10
  48.7 0.0 copy-start.11
  48.7 0.6 copy-done.9
  49.3 0.0 copy-done.10
  49.3 0.0 copy-done.11
  49.3 0.0 copy-start.7
  49.4 0.0 copy-start.8
  49.4 30.6 %exchange_middle.1 = (bf16[1024,128]{1,0:T(8,128)(2,1)S(1)}, bf16[1024,128]{1,0:T(8,128)(2,1)S(1)}) custom-call(bf16[1,128,256]{2,1,0:T(8,128)(2,1)S(1)} %get-tuple-element.22.final_ref, bf16[1024,128]{1,0:T(8,128)(2,1)S(1)} %get-tuple-element.23.gv_ref, bf16[1024,128]{1,0:T(8,128)(2,1)S(1)} %get-tuple-element.24.gg_ref, ...), custom_call_target="tpu_custom_call" | custom-call | flops 10000000000 | bytes 20000000 | tf_op jit(solution)/shard_map/exchange_middle/pallas_call | solution.py:504
  79.9 0.0 copy-done.7
  79.9 0.0 copy-done.8
  79.9 37.7 %output_scatter.1 = bf16[128,2048]{1,0:T(8,128)(2,1)S(1)} custom-call(bf16[1024,128]{1,0:T(8,128)(2,1)S(1)} %get-tuple-element.29.dm_ref, bf16[1024,128]{1,0:T(8,128)(2,1)S(1)} %get-tuple-element.30.cm_ref, bf16[128,2048]{1,0:T(8,128)(2,1)S(1)} %copy-done.7, bf16[128,2048]{1,0:T(8,128)(2,1)S(1)} %copy-done.8), custom_call_target="tpu_custom_call" | custom-call | flops 10000000000 | bytes 20000000 | tf_op jit(solution)/shard_map/output_scatter/pallas_call | solution.py:644
  117.6 0.8 copy.23
  (3 shorter events, 0.0 us)
Async XLA Ops:
  0.8 3.1 %copy-start.4 = (bf16[2048,128]{1,0:T(8,128)(2,1)S(1)}, bf16[2048,128]{1,0:T(8,128)(2,1)}, u32[]{:S(2)}) copy-start(bf16[2048,128]{1,0:T(8,128)(2,1)} %refs_4_.1) | copy-start | bytes 1572868
  1.1 2.8 %copy-start.3 = (bf16[2048,128]{1,0:T(8,128)(2,1)S(1)}, bf16[2048,128]{1,0:T(8,128)(2,1)}, u32[]{:S(2)}) copy-start(bf16[2048,128]{1,0:T(8,128)(2,1)} %refs_3_.1) | copy-start | bytes 1572868
  1.5 1.1 copy-start.13
  1.5 2.4 %copy-start = (bf16[1024,256]{1,0:T(8,128)(2,1)S(1)}, bf16[1024,256]{1,0:T(8,128)(2,1)}, u32[]{:S(2)}) copy-start(bf16[1024,256]{1,0:T(8,128)(2,1)} %refs_0_.1) | copy-start | bytes 1572868
  1.5 2.4 %copy-start.1 = (bf16[2048,128]{1,0:T(8,128)(2,1)S(1)}, bf16[2048,128]{1,0:T(8,128)(2,1)}, u32[]{:S(2)}) copy-start(bf16[2048,128]{1,0:T(8,128)(2,1)} %refs_1_.1) | copy-start | bytes 1572868
  1.5 2.4 %copy-start.2 = (bf16[2048,128]{1,0:T(8,128)(2,1)S(1)}, bf16[2048,128]{1,0:T(8,128)(2,1)}, u32[]{:S(2)}) copy-start(bf16[2048,128]{1,0:T(8,128)(2,1)} %refs_2_.1) | copy-start | bytes 1572868
  3.9 1.0 copy-start.5
  5.0 1.0 copy-start.6
  48.0 0.7 copy-start.12
  48.7 0.7 copy-start.9
  48.7 0.7 copy-start.10
  48.7 0.7 copy-start.11
  49.3 30.6 %copy-start.7 = (bf16[128,2048]{1,0:T(8,128)(2,1)S(1)}, bf16[128,2048]{1,0:T(8,128)(2,1)}, u32[]{:S(2)}) copy-start(bf16[128,2048]{1,0:T(8,128)(2,1)} %wd_ref.1) | copy-start | bytes 1572868
  49.4 30.6 %copy-start.8 = (bf16[128,2048]{1,0:T(8,128)(2,1)S(1)}, bf16[128,2048]{1,0:T(8,128)(2,1)}, u32[]{:S(2)}) copy-start(bf16[128,2048]{1,0:T(8,128)(2,1)} %wc_ref.1) | copy-start | bytes 1572868
where the time goes:
time: 119 us; the launch traced here: 118 us
  Pallas kernels  110 us (92%)
  local copies, waits for them, and re-layouts  6.33 us (5%)
  other arithmetic  1.2 us (1%)
    pallas_call x1, Pallas kernels, output_projection(): pl.pallas_call(output_kernel, out_shape=jax.ShapeDtypeStruct((rows, width...  37.7 us
    pallas_call x1, Pallas kernels, project(): pl.pallas_call(functools.partial(project_kernel, heads), out_shape=tuple(...  35.5 us
    pallas_call x1, Pallas kernels, middle(): pl.pallas_call(functools.partial(middle_kernel, heads, width), out_shape=...  30.6 us
    pallas_call x1, Pallas kernels, delta_rule(): pl.pallas_call(functools.partial(delta_kernel, heads, width), out_shape=(...  6.41 us
    unnamed x31, local copies, waits for them, and re-layouts  4.9 us

commit v1 on v0

v1 whole, which is shorter than its diff:
```python
import jax
import jax.numpy as jnp
from jax import lax
from jax.experimental import pallas as pl
from jax.experimental.pallas import tpu as pltpu
from jax.sharding import PartitionSpec as P

BLOCK = 128
AHEAD = 3
TINY_NORM = 1e-06
TINY_VAR = 1e-05
HIGHEST = lax.Precision.HIGHEST
MESH = pl.DeviceIdType.MESH
F32 = jnp.float32
BF16 = jnp.bfloat16
NX = 4
NZ = 8
NY = 4


def nt(a, b):
    return lax.dot_general(a, b, (((1,), (1,)), ((), ())), preferred_element_type=F32)


def mm(a, b):
    return jnp.dot(a.astype(BF16), b.astype(BF16), preferred_element_type=F32)


def compose(later, earlier):
    width = later.shape[0]
    moved = mm(later[:, :width], earlier)
    return jnp.concatenate(
        [moved[:, :width], moved[:, width:] + later[:, width:].astype(F32)], axis=1
    )


def layer_kernel(
    tok_hbm, wq_hbm, wk_hbm, wv_hbm, wdg_hbm, wgv_hbm, wgg_hbm, wcg_hbm, wb_hbm, wdec_hbm,
    rate_hbm, gain_hbm, taps_hbm, lng_hbm, lns_hbm, od_hbm, oc_hbm,
    out_ref,
    full, w_all, proj, gates_ref, wb_s, wdec_s, rate_s, gain_s, taps_s, tapf_s, lng_s, lns_s,
    wd, wc, lhs_s, corr_s, score_s, wt_s, tail_s, state_ref, outa_s, outb_s,
    xin, zs, zr, zs4, zr4, padded, filtered, halo_out, halo_in, sums_out, sums_in,
    cm_s, dsend, in_d, in_c, acc, gate_s,
    l_sem, r_send, r_recv, l_send, l_recv, fr_send, fr_recv, fl_send, fl_recv,
    b_send, b_recv, w1_send, w1_recv, w2_send, w2_recv, w3_send, w3_recv, wb_send, wb_recv,
    wd_send, wd_recv, x_send, x_recv, z_send, z_recv, h_send, h_recv, ln_send, ln_recv,
    c_send, c_recv, d_send, d_recv,
):
    rows, part = tok_hbm.shape
    chunks = rows // BLOCK
    width = gain_hbm.shape[1]
    halo = halo_in.shape[0]
    kernel = taps_hbm.shape[0]
    sp, place = NX * NZ, lax.axis_index("sp")
    me = lax.axis_index("tp")
    core, y = lax.rem(me, 2), me // 2
    x, z = lax.rem(place, NX), place // NX
    sibling = me + 1 - 2 * core

    def tp_at(o, p=0):
        side = core + p * (1 - 2 * core)
        return lax.rem(y + o + NY, NY) * 2 + side

    def sp_at(dz, dx):
        return lax.rem(z + dz + NZ, NZ) * NX + lax.rem(x + dx + NX, NX)

    barrier = pltpu.get_barrier_semaphore()

    def greet(**device):
        pl.semaphore_signal(barrier, inc=1, device_id=device, device_id_type=MESH)

    for o in (1, 2, 3):
        for p in range(2):
            greet(tp=tp_at(o, p))
    greet(tp=sibling)
    for j in range(1, NZ):
        greet(sp=sp_at(j, 0))
    for k in range(1, NX):
        greet(sp=sp_at(0, k))
    greet(sp=lax.rem(place + sp - 1, sp))

    def columns(owner):
        return pl.ds(pl.multiple_of(owner * part, part), part)

    def at(t):
        return pl.ds(pl.multiple_of(t * BLOCK, BLOCK), BLOCK)

    def load(i, src, dst):
        return pltpu.make_async_copy(src, dst, l_sem.at[i])

    loads = {"tok": load(0, tok_hbm, full.at[:, columns(me)]), "oc": load(1, oc_hbm, wc.at[0, :BLOCK, :])}
    for i, src in enumerate((wq_hbm, wk_hbm, wv_hbm, wdg_hbm, wgv_hbm, wgg_hbm, wcg_hbm)):
        loads[i] = load(2 + i, src, w_all.at[:, i * width : (i + 1) * width])
    loads["wb"] = load(9, wb_hbm, wb_s)
    loads["wdec"] = load(10, wdec_hbm, wdec_s)
    loads["rate"] = load(11, rate_hbm, rate_s)
    loads["gain"] = load(12, gain_hbm, gain_s)
    loads["taps"] = load(13, taps_hbm, taps_s)
    loads["lng"] = load(14, lng_hbm, lng_s)
    loads["lns"] = load(15, lns_hbm, lns_s)
    loads["od"] = load(16, od_hbm, wd.at[0, :BLOCK, :])
    for copy in loads.values():
        copy.start()

    def remote(src, dst, send, recv, **device):
        return pltpu.make_async_remote_copy(
            src_ref=src, dst_ref=dst, send_sem=send, recv_sem=recv,
            device_id=device, device_id_type=MESH,
        )

    def to_right(r):
        block = full.at[at(r), columns(me)]
        return remote(block, block, r_send.at[r], r_recv.at[r], tp=tp_at(1))

    def to_left(r):
        block = full.at[at(r), columns(me)]
        return remote(block, block, l_send.at[r], l_recv.at[r], tp=tp_at(-1))

    def half(r, i):
        return pl.ds(pl.multiple_of(r * BLOCK + i * (BLOCK // 2), BLOCK // 2), BLOCK // 2)

    def on_right(r):
        block = full.at[half(r, 0), columns(tp_at(-1))]
        return remote(block, block, fr_send.at[r], fr_recv.at[r], tp=tp_at(1))

    def on_left(r):
        block = full.at[half(r, 1), columns(tp_at(1))]
        return remote(block, block, fl_send.at[r], fl_recv.at[r], tp=tp_at(-1))

    def beside(o, r):
        block = full.at[at(r), columns(tp_at(o))]
        return remote(block, block, b_send.at[o, r], b_recv.at[o, r], tp=sibling)

    zrows = BLOCK // NZ
    xcols = wc.shape[2] // NX

    def wpiece(i):
        return (
            pl.ds(pl.multiple_of(lax.rem(z - i + NZ, NZ) * zrows, zrows), zrows),
            pl.ds(pl.multiple_of(x * xcols, xcols), xcols),
        )

    def w_first(o):
        a, b = wpiece(0)
        return remote(
            wc.at[0, a, b], wc.at[NY - o, a, b], w1_send.at[o - 1], w1_recv.at[o - 1], tp=tp_at(o)
        )

    def w_second(j):
        a, b = wpiece(0)
        block = wc.at[pl.ds(1, NY - 1), a, b]
        return remote(block, block, w2_send.at[j - 1], w2_recv.at[j - 1], sp=sp_at(j, 0))

    def w_third(i, k):
        a, b = wpiece(i)
        block = wc.at[pl.ds(1, NY - 1), a, b]
        return remote(block, block, w3_send.at[i, k - 1], w3_recv.at[i, k - 1], sp=sp_at(0, k))

    def w_beside(i, ref):
        return remote(
            ref.at[:, pl.ds(0, BLOCK), :], ref.at[:, pl.ds(BLOCK, BLOCK), :],
            wb_send.at[i], wb_recv.at[i], tp=sibling,
        )

    hb = BLOCK // 2

    def d_right(i):
        return remote(
            wd.at[0, pl.ds(i * hb, hb), :], wd.at[3, pl.ds(i * hb, hb), :],
            wd_send.at[i], wd_recv.at[i], tp=tp_at(1),
        )

    def d_left(i):
        return remote(
            wd.at[0, pl.ds((1 - i) * hb, hb), :], wd.at[1, pl.ds((1 - i) * hb, hb), :],
            wd_send.at[2 + i], wd_recv.at[2 + i], tp=tp_at(-1),
        )

    def d_on_right():
        return remote(
            wd.at[3, pl.ds(0, hb), :], wd.at[2, pl.ds(0, hb), :],
            wd_send.at[4], wd_recv.at[4], tp=tp_at(1),
        )

    def d_on_left():
        return remote(
            wd.at[1, pl.ds(hb, hb), :], wd.at[2, pl.ds(hb, hb), :],
            wd_send.at[5], wd_recv.at[5], tp=tp_at(-1),
        )

    loads["tok"].wait()
    loads["oc"].wait()
    pl.semaphore_wait(barrier, 7 + NZ - 1 + NX - 1 + 1)
    for o in (2, 1, 3):
        w_first(o).start()
    for r in range(AHEAD):
        to_right(r).start()
        to_left(r).start()

    def own_beside(r, carry):
        beside(0, r).start()
        return carry

    lax.fori_loop(0, chunks, own_beside, 0)

    loads["wb"].wait()
    loads["wdec"].wait()
    loads["rate"].wait()
    heads = wb_s.shape[0]
    pick = lax.broadcasted_iota(jnp.int32, wb_s.shape, 0) == me
    beta_row = jnp.sum(jnp.where(pick, wb_s[...].astype(F32), 0.0), axis=0, keepdims=True)
    decay_row = jnp.sum(jnp.where(pick, wdec_s[...].astype(F32), 0.0), axis=0, keepdims=True)
    sub_id = lax.broadcasted_iota(jnp.int32, (BLOCK, BLOCK), 0)
    for b in range(2 * NY * part // BLOCK):
        cut = slice(b * BLOCK, (b + 1) * BLOCK)
        tall = jnp.where(sub_id == 0, beta_row[:, cut], jnp.where(sub_id == 1, decay_row[:, cut], 0.0))
        w_all[cut, 7 * width : 8 * width] = tall.T.astype(BF16)
    lane8 = lax.broadcasted_iota(jnp.int32, (1, heads), 1)
    rate = jnp.exp(
        jnp.sum(jnp.where(lane8 == me, rate_s[...], 0.0), axis=1, keepdims=True)
    )
    for i in range(7):
        loads[i].wait()
    loads["taps"].wait()
    tapf_s[:kernel, :] = taps_s[...].astype(F32)

    def arrive(r):
        to_right(r).wait_recv()
        to_left(r).wait_recv()
        on_right(r).start()
        on_left(r).start()
        beside(3, r).start()
        beside(1, r).start()

        @pl.when(r + AHEAD < chunks)
        def _():
            to_right(r + AHEAD).start()
            to_left(r + AHEAD).start()

    def arrive_far(r):
        on_right(r).wait_recv()
        on_left(r).wait_recv()
        beside(2, r).start()

    def w_pass(r):
        w_second(r).wait_recv()
        for k in (2, 1, 3):
            w_third(r, k).start()

    def chunk(r):
        for o in range(NY):
            beside(o, r).wait_recv()
        here = at(r)
        squares = jnp.zeros((BLOCK, 1), F32)
        for b in range(2 * NY):
            piece = full[here, b * part : (b + 1) * part].astype(F32)
            squares = squares + jnp.sum(piece * piece, axis=1, keepdims=True)
        inv_rms = lax.rsqrt(squares / (part * 2 * NY) + TINY_NORM)
        for j in range(4):
            summed = jnp.dot(
                full[here, :], w_all[:, j * 256 : (j + 1) * 256], preferred_element_type=F32
            )
            summed = summed * inv_rms
            proj[2 * j, here, :] = summed[:, :width].astype(BF16)
            if j < 3:
                proj[2 * j + 1, here, :] = summed[:, width:].astype(BF16)
            else:
                raw = summed[:, width:]
                lane = lax.broadcasted_iota(jnp.int32, raw.shape, 1)
                softplus = jnp.maximum(raw, 0.0) + jnp.log1p(jnp.exp(-jnp.abs(raw)))
                gates_ref[here, :] = jnp.where(
                    lane == 0, jax.nn.sigmoid(raw), jnp.where(lane == 1, -rate * softplus, 0.0)
                )

    row_id = lax.broadcasted_iota(jnp.int32, (BLOCK, BLOCK), 0)
    col_id = lax.broadcasted_iota(jnp.int32, (BLOCK, BLOCK), 1)
    causal = row_id >= col_id
    strict = row_id > col_id
    differ = row_id ^ col_id
    eye = jnp.where(row_id == col_id, 1.0, 0.0)
    tril = jnp.where(causal, 1.0, 0.0)
    ident = jnp.concatenate([eye, jnp.zeros((width, width), F32)], axis=1)

    def prepare(c):
        here = slice(c * BLOCK, (c + 1) * BLOCK)
        gates = gates_ref[here, :]
        sums = jnp.dot(tril, gates, precision=HIGHEST, preferred_element_type=F32)
        q, k = proj[0, here, :], proj[1, here, :]
        v = proj[2, here, :].astype(F32)
        kf, qf = k.astype(F32), q.astype(F32)
        ik = lax.rsqrt(jnp.sum(kf * kf, axis=-1, keepdims=True) + TINY_NORM)
        iq = lax.rsqrt(jnp.sum(qf * qf, axis=-1, keepdims=True) + TINY_NORM)
        iq = iq * width ** (-0.5)
        beta = gates[:, 0:1]
        log_sum = sums[:, 1:2]
        log_full = jnp.broadcast_to(log_sum, (BLOCK, BLOCK))
        spread = log_full - log_full.T
        damp = jnp.where(causal, jnp.exp(jnp.where(causal, spread, 0.0)), 0.0)
        damp = damp * jnp.broadcast_to(ik, (BLOCK, BLOCK)).T
        lower = jnp.where(strict, nt(k, k) * damp * (beta * ik), 0.0)
        score_s[here, :] = (nt(q, k) * damp * iq).astype(BF16)
        grow = jnp.exp(log_sum)
        right = jnp.concatenate([v * beta, kf * (beta * ik * grow)], axis=1)
        tail = log_full[BLOCK - 1 : BLOCK, :]
        weighted = kf * (ik * jnp.exp(tail[:, :1] - log_sum))
        wt_s[c] = weighted.T.astype(BF16)
        tail_s[c] = jnp.broadcast_to(jnp.exp(tail), (8, BLOCK))
        lhs_s[c, BLOCK:, :] = (qf * (iq * grow)).astype(BF16)
        return [c, lower, right, eye - jnp.where(differ == 1, lower, 0.0)]

    def advance(c, carry):
        both = mm(lhs_s[c], state_ref[...])
        first = both[:BLOCK]
        fresh = jnp.concatenate(
            [-first[:, :width], corr_s[at(c), :] - first[:, width:]], axis=1
        ).astype(BF16)
        decay = tail_s[c][:1, :]
        decay = jnp.concatenate([decay, decay], axis=1)
        state_ref[...] = state_ref[...] * decay + mm(wt_s[c], fresh)
        out = both[BLOCK:] + mm(score_s[at(c), :], fresh)
        outa_s[at(c), :] = out[:, :width].astype(BF16)
        outb_s[at(c), :] = out[:, width:]
        return carry

    def delta_group(first, count):
        chains = [prepare(first + i) for i in range(count)]
        size = 2
        while size < BLOCK:
            level = (differ >= size) & (differ < 2 * size)
            moved = [mm(jnp.where(level, ch[1], 0.0), ch[3]) for ch in chains]
            for ch, part_ in zip(chains, moved):
                ch[3] = ch[3] - mm(ch[3], part_)
            size *= 2
        for c, lower, right, inverse in chains:
            solved = mm(inverse, right)
            corr_s[c * BLOCK : (c + 1) * BLOCK, :] = solved[:, :width]
            lhs_s[c, :BLOCK, :] = solved[:, width:].astype(BF16)
        lax.fori_loop(first, first + count, advance, 0)

    state_ref[...] = ident
    for o in (1, 2, 3):
        w_first(o).wait_recv()
    for j in range(1, NZ):
        w_second(j).start()
    for k in (2, 1, 3):
        w_third(0, k).start()
    arrive(0)
    arrive(1)
    arrive_far(0)
    w_pass(1)

    def steady(r, carry):
        arrive(r)
        arrive_far(r - 1)
        chunk(r - 2)
        w_pass(r)
        return carry

    lax.fori_loop(2, 6, steady, 0)
    arrive(6)
    arrive_far(5)
    delta_group(0, 4)
    w_pass(6)
    arrive(7)
    arrive_far(6)
    loads["od"].wait()
    d_right(0).start()
    d_left(0).start()
    w_pass(7)

    def late(r, carry):
        @pl.when(r == 6)
        def _():
            arrive_far(7)

        chunk(r)
        return carry

    lax.fori_loop(4, 8, late, 0)

    def unit(t):
        value = proj[4, at(t), :].astype(F32)
        units = (value * jax.nn.sigmoid(proj[5, at(t), :].astype(F32))).astype(BF16)
        padded[pl.ds(pl.multiple_of(t * BLOCK + halo, halo), BLOCK), :] = units.astype(F32)
        return units

    units = unit(chunks - 1)
    halo_out[...] = units[BLOCK - halo :, :]
    halo_copy = remote(
        halo_out, halo_in, h_send.at[0], h_recv.at[0], sp=lax.rem(place + 1, sp)
    )

    @pl.when(place + 1 < sp)
    def _():
        halo_copy.start()

    delta_group(4, 4)

    xin[0] = state_ref[...].astype(BF16)

    def x_copy(k):
        return remote(xin.at[0], xin.at[k], x_send.at[k - 1], x_recv.at[k - 1], sp=sp_at(0, k))

    for k in (2, 1, 3):
        x_copy(k).start()

    def unit_loop(t, carry):
        unit(t)
        return carry

    lax.fori_loop(0, chunks - 1, unit_loop, 0)

    def conv(t, carry):
        total = jnp.zeros((BLOCK, width), F32)
        for j in range(kernel):
            start = t * BLOCK + (halo - kernel + 1 + j)
            total = total + padded[pl.ds(start, BLOCK), :] * tapf_s[j : j + 1, :]
        filtered[at(t), :] = total
        first = jnp.sum(total, axis=1, keepdims=True)
        second = jnp.sum(total * total, axis=1, keepdims=True)
        turned = jnp.where(col_id == 0, first, jnp.where(col_id == 1, second, 0.0)).T
        sums_out[pl.ds(t, 1), :] = turned[0:1, :]
        sums_out[pl.ds(t + 8, 1), :] = turned[1:2, :]
        return carry

    lax.fori_loop(1, chunks, conv, 0)

    for k in (1, 2, 3):
        x_copy(k).wait_recv()

    def piece(i):
        return xin[lax.rem(x - i + NX, NX)]

    p0, p1, p2, p3 = (piece(i) for i in range(NX))
    w2 = compose(p1, p0)
    pair = compose(p3, p2)
    group = compose(pair, w2)
    w3 = compose(p2, w2)
    inner = jnp.where(
        x == 0, ident, jnp.where(x == 1, p0.astype(F32), jnp.where(x == 2, w2, w3))
    ).astype(BF16)
    zs[0] = group.astype(BF16)

    def z_copy(i):
        return remote(zs.at[i], zr.at[i], z_send.at[i], z_recv.at[i], sp=sp_at(i + 1, 0))

    last_copy = remote(zs4, zr4, z_send.at[2], z_recv.at[2], sp=sp_at(4, 0))

    @pl.when(z + 1 < NZ)
    def _():
        z_copy(0).start()

    for i in range(2):

        @pl.when(z < i + 1)
        def _(i=i):
            zr[i] = ident.astype(BF16)

    @pl.when(z < 4)
    def _():
        zr4[...] = jnp.zeros(zr4.shape, BF16)

    @pl.when(place >= 1)
    def _():
        halo_copy.wait_recv()

    @pl.when(place < 1)
    def _():
        halo_in[...] = jnp.zeros(halo_in.shape, BF16)

    padded[:halo, :] = halo_in[...].astype(F32)
    conv(0, 0)

    def ln_copy(o, p):
        i = 2 * o + p - 1
        return remote(
            sums_out, sums_in.at[i], ln_send.at[i], ln_recv.at[i], tp=tp_at(o, p)
        )

    others = [(2, 0), (2, 1), (1, 0), (1, 1), (3, 0), (3, 1), (0, 1)]
    for o, p in others:
        ln_copy(o, p).start()
    d_right(1).start()
    d_left(1).start()

    @pl.when(z >= 1)
    def _():
        z_copy(0).wait_recv()

    e1 = zr[0]
    i2 = compose(zs[0], e1)
    zs[1] = i2.astype(BF16)

    @pl.when(z + 2 < NZ)
    def _():
        z_copy(1).start()

    for o, p in others:
        ln_copy(o, p).wait_recv()
    loads["lng"].wait()
    loads["lns"].wait()
    loads["gain"].wait()
    sums = sums_out[...]
    for i in range(7):
        sums = sums + sums_in[i]
    sums = jnp.concatenate([sums, jnp.zeros((BLOCK - 16, BLOCK), F32)], axis=0).T
    channels = width * 2 * NY
    center_all = sums[:, 0:8] / channels
    variance = jnp.maximum(sums[:, 8:16] / channels - center_all * center_all, 0.0)
    scale_all = lax.rsqrt(variance + TINY_VAR)
    for t in range(chunks):
        here = slice(t * BLOCK, (t + 1) * BLOCK)
        normed = (filtered[here, :] - center_all[:, t : t + 1]) * scale_all[:, t : t + 1]
        normed = normed * lng_s[...] + lns_s[...]
        gate = proj[6, here, :].astype(F32)
        cm_s[here, :] = (jax.nn.silu(normed) * jax.nn.silu(gate)).astype(BF16)

    def c_copy(o, p):
        i = 2 * o + p - 1
        return remote(
            cm_s.at[at(tp_at(o, p)), :],
            in_c.at[(NY - o) % NY, :, pl.ds(p * width, width)],
            c_send.at[i], c_recv.at[i], tp=tp_at(o, p),
        )

    for o, p in others:
        c_copy(o, p).start()
    in_c[0, :, :width] = cm_s[at(me), :]
    for i in range(NZ):
        for k in range(1, NX):
            w_third(i, k).wait_recv()
    w_beside(0, wc).start()

    @pl.when(z >= 2)
    def _():
        z_copy(1).wait_recv()

    n2 = zr[1]
    i2b = zs[1]
    zs4[...] = (mm(i2b[:, :width], n2[:, width:]) + i2b[:, width:].astype(F32)).astype(BF16)

    @pl.when(z + 4 < NZ)
    def _():
        last_copy.start()

    e3 = compose(e1, n2)
    reach = compose(inner, e3)
    d_right(0).wait_recv()
    d_left(0).wait_recv()
    d_on_right().start()
    d_on_left().start()

    for t in range(chunks):
        here = slice(t * BLOCK, (t + 1) * BLOCK)
        gate_s[here, :] = gain_s[...] * jax.nn.silu(proj[3, here, :].astype(F32))

    w_beside(0, wc).wait_recv()
    for o, p in others:
        c_copy(o, p).wait_recv()
    step = 512
    for n in range(out_ref.shape[1] // step):
        cut = slice(n * step, (n + 1) * step)
        total = jnp.zeros((BLOCK, step), F32)
        for d in range(NY):
            total = total + jnp.dot(in_c[d], wc[d, :, cut], preferred_element_type=F32)
        acc[:, cut] = total

    @pl.when(z >= 4)
    def _():
        last_copy.wait_recv()

    carried = (mm(reach[:, :width], zr4[...]) + reach[:, width:]).astype(BF16)

    def d_copy(o, p):
        i = 2 * o + p - 1
        return remote(
            dsend.at[i], in_d.at[(NY - o) % NY, :, pl.ds(p * width, width)],
            d_send.at[i], d_recv.at[i], tp=tp_at(o, p),
        )

    for batch in (others[:2], others[2:6], [(0, 1), (0, 0)]):
        places = [at(tp_at(o, p)) for o, p in batch]
        results = [outb_s[pos, :] + mm(outa_s[pos, :], carried) for pos in places]
        scales = [
            lax.rsqrt(jnp.mean(res * res, axis=-1, keepdims=True) + TINY_NORM) for res in results
        ]
        mixed = [
            (res * sc * gate_s[pos, :]).astype(BF16)
            for res, sc, pos in zip(results, scales, places)
        ]
        for (o, p), value in zip(batch, mixed):
            if o == 0 and p == 0:
                in_d[0, :, :width] = value
            else:
                dsend[2 * o + p - 1] = value
        for o, p in batch:
            if o or p:
                d_copy(o, p).start()

    d_right(1).wait_recv()
    d_left(1).wait_recv()
    d_on_right().wait_recv()
    d_on_left().wait_recv()
    w_beside(1, wd).start()
    w_beside(1, wd).wait_recv()
    for group_at in ((0,), (3, 1), (2,)):
        for d in group_at:
            o = (NY - d) % NY
            for p in range(2):
                if o or p:
                    d_copy(o, p).wait_recv()
        for n in range(out_ref.shape[1] // step):
            cut = slice(n * step, (n + 1) * step)
            total = acc[:, cut]
            for d in group_at:
                total = total + jnp.dot(in_d[d], wd[d, :, cut], preferred_element_type=F32)
            if group_at == (2,):
                out_ref[:, cut] = total.astype(BF16)
            else:
                acc[:, cut] = total

    def drain(r, carry):
        to_right(r).wait_send()
        to_left(r).wait_send()
        on_right(r).wait_send()
        on_left(r).wait_send()
        for o in range(NY):
            beside(o, r).wait_send()
        for k in range(1, NX):
            w_third(r, k).wait_send()
        return carry

    lax.fori_loop(0, chunks, drain, 0)
    for o in (1, 2, 3):
        w_first(o).wait_send()
    for j in range(1, NZ):
        w_second(j).wait_send()
    for i in range(2):
        d_right(i).wait_send()
        d_left(i).wait_send()
    d_on_right().wait_send()
    d_on_left().wait_send()
    w_beside(0, wc).wait_send()
    w_beside(1, wd).wait_send()
    for k in (1, 2, 3):
        x_copy(k).wait_send()

    @pl.when(place + 1 < sp)
    def _():
        halo_copy.wait_send()

    for i in range(2):

        @pl.when(z + i + 1 < NZ)
        def _(i=i):
            z_copy(i).wait_send()

    @pl.when(z + 4 < NZ)
    def _():
        last_copy.wait_send()

    for o, p in others:
        ln_copy(o, p).wait_send()
        c_copy(o, p).wait_send()
        d_copy(o, p).wait_send()


def local(
    tokens, w_query, w_key, w_value, w_delta_gate, w_glu_value, w_glu_gate, w_conv_gate,
    w_beta, w_decay, decay_log, head_gain, conv_taps, ln_gain, ln_shift, out_delta, out_conv,
):
    rows, part = tokens.shape
    depth, width = w_query.shape
    wide = out_delta.shape[1]
    heads = w_beta.shape[1]
    chunks = rows // BLOCK
    kernel = conv_taps.shape[0]
    halo = (kernel - 1 + 31) // 32 * 32
    hbm = pl.BlockSpec(memory_space=pltpu.HBM)
    dma = pltpu.SemaphoreType.DMA
    vm = pltpu.VMEM
    return pl.pallas_call(
        layer_kernel,
        out_shape=jax.ShapeDtypeStruct((BLOCK, wide), BF16),
        in_specs=[hbm] * 17,
        out_specs=pl.BlockSpec(memory_space=pltpu.VMEM),
        scratch_shapes=[
            vm((rows, depth), BF16),
            vm((depth, 8 * width), BF16),
            vm((7, rows, width), BF16),
            vm((rows, width), F32),
            vm((heads, depth), BF16),
            vm((heads, depth), BF16),
            vm((1, heads), F32),
            vm((1, width), F32),
            vm((kernel, width), BF16),
            vm((32, width), F32),
            vm((1, width), F32),
            vm((1, width), F32),
            vm((NY, 2 * BLOCK, wide), BF16),
            vm((NY, 2 * BLOCK, wide), BF16),
            vm((chunks, 2 * BLOCK, width), BF16),
            vm((rows, width), F32),
            vm((rows, BLOCK), BF16),
            vm((chunks, width, BLOCK), BF16),
            vm((chunks, 8, BLOCK), F32),
            vm((width, 2 * width), F32),
            vm((rows, width), BF16),
            vm((rows, width), F32),
            vm((NX, width, 2 * width), BF16),
            vm((2, width, 2 * width), BF16),
            vm((2, width, 2 * width), BF16),
            vm((width, width), BF16),
            vm((width, width), BF16),
            vm((halo + rows, width), F32),
            vm((rows, width), F32),
            vm((halo, width), BF16),
            vm((halo, width), BF16),
            vm((16, BLOCK), F32),
            vm((7, 16, BLOCK), F32),
            vm((rows, width), BF16),
            vm((7, BLOCK, width), BF16),
            vm((NY, BLOCK, 2 * width), BF16),
            vm((NY, BLOCK, 2 * width), BF16),
            vm((BLOCK, wide), F32),
            vm((rows, width), F32),
            dma((17,)),
            dma((chunks,)), dma((chunks,)), dma((chunks,)), dma((chunks,)),
            dma((chunks,)), dma((chunks,)), dma((chunks,)), dma((chunks,)),
            dma((NY, chunks)), dma((NY, chunks)),
            dma((NY - 1,)), dma((NY - 1,)),
            dma((NZ - 1,)), dma((NZ - 1,)),
            dma((NZ, NX - 1)), dma((NZ, NX - 1)),
            dma((2,)), dma((2,)),
            dma((6,)), dma((6,)),
            dma((NX - 1,)), dma((NX - 1,)),
            dma((3,)), dma((3,)),
            dma((1,)), dma((1,)),
            dma((7,)), dma((7,)),
            dma((7,)), dma((7,)),
            dma((7,)), dma((7,)),
        ],
        compiler_params=pltpu.CompilerParams(
            collective_id=0, has_side_effects=True, vmem_limit_bytes=60 * 1024 * 1024
        ),
        cost_estimate=pl.CostEstimate(
            flops=10_000_000_000, bytes_accessed=20_000_000, transcendentals=0
        ),
        name="layer",
    )(
        tokens, w_query, w_key, w_value, w_delta_gate, w_glu_value, w_glu_gate, w_conv_gate,
        w_beta.T, w_decay.T, decay_log[None, :], head_gain[None, :], conv_taps,
        ln_gain[None, :], ln_shift[None, :], out_delta, out_conv,
    )


def solution(mesh):
    return jax.shard_map(
        local,
        mesh=mesh,
        in_specs=(
            P("sp", "tp"), P(None, "tp"), P(None, "tp"), P(None, "tp"), P(None, "tp"),
            P(None, "tp"), P(None, "tp"), P(None, "tp"), P(), P(), P(), P(), P(None, "tp"),
            P("tp"), P("tp"), P("tp", None), P("tp", None),
        ),
        out_specs=P(("sp", "tp"), None),
        check_vma=False,
    )
```

time: 119 us -> 79.7 us (0.67)
  Pallas kernels: 110 us -> 77.7 us
  local copies, waits for them, and re-layouts: 6.33 us -> 1.88 us
  other arithmetic: 1.2 us -> 0 us
    pallas_call x4 -> x1, Pallas kernels: 110 us -> 77.7 us  [local(): pl.pallas_call(layer_kernel, out_shape=jax.ShapeDtypeStruct((BLOCK, wide)...]
    unnamed x31 -> x1, local copies, waits for them, and re-layouts: 4.9 us -> 1.88 us
    dynamic_slice x2 -> x0, local copies, waits for them, and re-layouts: 1.35 us -> none  [the longest x1 0.79 us: local(): lax.dynamic_slice_in_dim(w_decay, first_head, heads_here, 1)]
where the time goes in v1:
time: 79.7 us; the launch traced here: 79.6 us
  Pallas kernels  77.7 us (97%)
  local copies, waits for them, and re-layouts  1.88 us (2%)
    pallas_call x1, Pallas kernels, local(): pl.pallas_call(layer_kernel, out_shape=jax.ShapeDtypeStruct((BLOCK, wide)...  77.7 us
    unnamed x1, local copies, waits for them, and re-layouts  1.88 us

profile of v1, /device:TPU:1, one launch (start us, length us, event | category | flops | bytes accessed | tf_op | source)
XLA Modules:
  0.0 79.6 jit_solution(12921629367853319724)
XLA Ops:
  0.0 77.7 %layer.1 = bf16[128,2048]{1,0:T(8,128)(2,1)} custom-call(bf16[1024,256]{1,0:T(8,128)(2,1)} %tok_hbm.1, bf16[2048,128]{1,0:T(8,128)(2,1)} %wq_hbm.1, bf16[2048,128]{1,0:T(8,128)(2,1)} %wk_hbm.1, bf16[2048,128]{1,0:T(8,128)(2,1)} %wv_hbm.1, bf16[2048,128]{1,0:T(8,128)(2,1)} %wdg_hbm.1, bf16[2048,128]{1,0:T(8,128)(2,1)} %wgv_hbm.1, bf16[2048,128]{1,0:T(8,128)(2,1)} %wgg_hbm.1, ...), custom_call_target="tpu_custom_call" | custom-call | flops 10000000000 | bytes 20000000 | tf_op jit(solution)/shard_map/layer/pallas_call | solution.py:683
  77.7 1.9 %copy.19 = bf16[128,2048]{1,0:T(8,128)(2,1)} copy(bf16[128,2048]{1,0:T(8,128)(2,1)} %layer.1) | data formatting | bytes 1048576

commit v2 on v1

--- a/solution.py
+++ b/solution.py
@@ -37,15 +37,15 @@
 def layer_kernel(
     tok_hbm, wq_hbm, wk_hbm, wv_hbm, wdg_hbm, wgv_hbm, wgg_hbm, wcg_hbm, wb_hbm, wdec_hbm,
     rate_hbm, gain_hbm, taps_hbm, lng_hbm, lns_hbm, od_hbm, oc_hbm,
-    out_ref,
-    full, w_all, proj, gates_ref, wb_s, wdec_s, rate_s, gain_s, taps_s, tapf_s, lng_s, lns_s,
+    out_hbm,
+    out_ref, full, w_all, proj, gates_ref, wb_s, wdec_s, rate_s, gain_s, taps_s, tapf_s, lng_s, lns_s,
     wd, wc, lhs_s, corr_s, score_s, wt_s, tail_s, state_ref, outa_s, outb_s,
     xin, zs, zr, zs4, zr4, padded, filtered, halo_out, halo_in, sums_out, sums_in,
     cm_s, dsend, in_d, in_c, acc, gate_s,
     l_sem, r_send, r_recv, l_send, l_recv, fr_send, fr_recv, fl_send, fl_recv,
     b_send, b_recv, w1_send, w1_recv, w2_send, w2_recv, w3_send, w3_recv, wb_send, wb_recv,
     wd_send, wd_recv, x_send, x_recv, z_send, z_recv, h_send, h_recv, ln_send, ln_recv,
-    c_send, c_recv, d_send, d_recv,
+    c_send, c_recv, d_send, d_recv, o_sem,
 ):
     rows, part = tok_hbm.shape
     chunks = rows // BLOCK
@@ -157,10 +157,16 @@
         block = wc.at[pl.ds(1, NY - 1), a, b]
         return remote(block, block, w3_send.at[i, k - 1], w3_recv.at[i, k - 1], sp=sp_at(0, k))
 
-    def w_beside(i, ref):
-        return remote(
-            ref.at[:, pl.ds(0, BLOCK), :], ref.at[:, pl.ds(BLOCK, BLOCK), :],
-            wb_send.at[i], wb_recv.at[i], tp=sibling,
+    def w_beside():
+        return remote(
+            wc.at[:, pl.ds(0, BLOCK), :], wc.at[:, pl.ds(BLOCK, BLOCK), :],
+            wb_send.at[NY], wb_recv.at[NY], tp=sibling,
+        )
+
+    def d_beside(d):
+        return remote(
+            wd.at[d, pl.ds(0, BLOCK), :], wd.at[d, pl.ds(BLOCK, BLOCK), :],
+            wb_send.at[d], wb_recv.at[d], tp=sibling,
         )
 
     hb = BLOCK // 2
@@ -323,10 +329,12 @@
         outb_s[at(c), :] = out[:, width:]
         return carry
 
-    def delta_group(first, count):
+    def delta_group(first, count, pauses=()):
         chains = [prepare(first + i) for i in range(count)]
         size = 2
         while size < BLOCK:
+            if size in pauses:
+                yield
             level = (differ >= size) & (differ < 2 * size)
             moved = [mm(jnp.where(level, ch[1], 0.0), ch[3]) for ch in chains]
             for ch, part_ in zip(chains, moved):
@@ -358,26 +366,25 @@
         return carry
 
     lax.fori_loop(2, 6, steady, 0)
+    early = delta_group(0, 4, (8, 64))
     arrive(6)
     arrive_far(5)
-    delta_group(0, 4)
+    next(early)
+    chunk(4)
     w_pass(6)
     arrive(7)
+    loads["od"].wait()
+    for i in range(2):
+        d_right(i).start()
+        d_left(i).start()
     arrive_far(6)
-    loads["od"].wait()
-    d_right(0).start()
-    d_left(0).start()
+    next(early)
+    chunk(5)
     w_pass(7)
-
-    def late(r, carry):
-        @pl.when(r == 6)
-        def _():
-            arrive_far(7)
-
-        chunk(r)
-        return carry
-
-    lax.fori_loop(4, 8, late, 0)
+    arrive_far(7)
+    list(early)
+    chunk(6)
+    chunk(7)
 
     def unit(t):
         value = proj[4, at(t), :].astype(F32)
@@ -395,7 +402,7 @@
     def _():
         halo_copy.start()
 
-    delta_group(4, 4)
+    list(delta_group(4, 4))
 
     xin[0] = state_ref[...].astype(BF16)
 
@@ -409,6 +416,10 @@
         unit(t)
         return carry
 
+    for i in range(NZ):
+        for k in range(1, NX):
+            w_third(i, k).wait_recv()
+    w_beside().start()
     lax.fori_loop(0, chunks - 1, unit_loop, 0)
 
     def conv(t, carry):
@@ -425,6 +436,13 @@
         return carry
 
     lax.fori_loop(1, chunks, conv, 0)
+    for i in range(2):
+        d_right(i).wait_recv()
+        d_left(i).wait_recv()
+    d_on_right().start()
+    d_on_left().start()
+    for d in (0, 1, 3):
+        d_beside(d).start()
 
     for k in (1, 2, 3):
         x_copy(k).wait_recv()
@@ -442,14 +460,27 @@
     ).astype(BF16)
     zs[0] = group.astype(BF16)
 
-    def z_copy(i):
-        return remote(zs.at[i], zr.at[i], z_send.at[i], z_recv.at[i], sp=sp_at(i + 1, 0))
-
-    last_copy = remote(zs4, zr4, z_send.at[2], z_recv.at[2], sp=sp_at(4, 0))
-
-    @pl.when(z + 1 < NZ)
-    def _():
-        z_copy(0).start()
+    def z_copy(i, b):
+        cut = pl.ds(b * width, width)
+        return remote(
+            zs.at[i, :, cut], zr.at[i, :, cut],
+            z_send.at[2 * i + b], z_recv.at[2 * i + b], sp=sp_at(i + 1, 0),
+        )
+
+    last_copy = remote(zs4, zr4, z_send.at[4], z_recv.at[4], sp=sp_at(4, 0))
+
+    def z_start(i, b):
+        @pl.when(z + i + 1 < NZ)
+        def _():
+            z_copy(i, b).start()
+
+    def z_wait(i, b):
+        @pl.when(z >= i + 1)
+        def _():
+            z_copy(i, b).wait_recv()
+
+    z_start(0, 1)
+    z_start(0, 0)
 
     for i in range(2):
 
@@ -481,20 +512,37 @@
     others = [(2, 0), (2, 1), (1, 0), (1, 1), (3, 0), (3, 1), (0, 1)]
     for o, p in others:
         ln_copy(o, p).start()
-    d_right(1).start()
-    d_left(1).start()
-
-    @pl.when(z >= 1)
-    def _():
-        z_copy(0).wait_recv()
-
+    def drain(r, carry):
+        to_right(r).wait_send()
+        to_left(r).wait_send()
+        on_right(r).wait_send()
+        on_left(r).wait_send()
+        for o in range(NY):
+            beside(o, r).wait_send()
+        for k in range(1, NX):
+            w_third(r, k).wait_send()
+        return carry
+
+    lax.fori_loop(0, chunks, drain, 0)
+    for o in (1, 2, 3):
+        w_first(o).wait_send()
+    for j in range(1, NZ):
+        w_second(j).wait_send()
+    for k in (1, 2, 3):
+        x_copy(k).wait_send()
+
+    def left(i):
+        return zs[i][:, :width]
+
+    z_wait(0, 1)
+    zs[1, :, width:] = (
+        mm(left(0), zr[0, :, width:]) + zs[0, :, width:].astype(F32)
+    ).astype(BF16)
+    z_start(1, 1)
+    z_wait(0, 0)
     e1 = zr[0]
-    i2 = compose(zs[0], e1)
-    zs[1] = i2.astype(BF16)
-
-    @pl.when(z + 2 < NZ)
-    def _():
-        z_copy(1).start()
+    zs[1, :, :width] = mm(left(0), e1[:, :width]).astype(BF16)
+    z_start(1, 0)
 
     for o, p in others:
         ln_copy(o, p).wait_recv()
@@ -527,39 +575,35 @@
     for o, p in others:
         c_copy(o, p).start()
     in_c[0, :, :width] = cm_s[at(me), :]
-    for i in range(NZ):
-        for k in range(1, NX):
-            w_third(i, k).wait_recv()
-    w_beside(0, wc).start()
-
-    @pl.when(z >= 2)
-    def _():
-        z_copy(1).wait_recv()
-
-    n2 = zr[1]
-    i2b = zs[1]
-    zs4[...] = (mm(i2b[:, :width], n2[:, width:]) + i2b[:, width:].astype(F32)).astype(BF16)
+    d_on_right().wait_recv()
+    d_on_left().wait_recv()
+    d_beside(2).start()
+    z_wait(1, 1)
+    zs4[...] = (mm(left(1), zr[1, :, width:]) + zs[1, :, width:].astype(F32)).astype(BF16)
 
     @pl.when(z + 4 < NZ)
     def _():
         last_copy.start()
 
-    e3 = compose(e1, n2)
+    z_wait(1, 0)
+    e3 = compose(e1, zr[1])
     reach = compose(inner, e3)
-    d_right(0).wait_recv()
-    d_left(0).wait_recv()
-    d_on_right().start()
-    d_on_left().start()
 
     for t in range(chunks):
         here = slice(t * BLOCK, (t + 1) * BLOCK)
         gate_s[here, :] = gain_s[...] * jax.nn.silu(proj[3, here, :].astype(F32))
 
-    w_beside(0, wc).wait_recv()
+    w_beside().wait_recv()
     for o, p in others:
         c_copy(o, p).wait_recv()
     step = 512
-    for n in range(out_ref.shape[1] // step):
+    cuts = out_ref.shape[1] // step
+
+    def out_copy(n):
+        cut = pl.ds(n * step, step)
+        return pltpu.make_async_copy(out_ref.at[:, cut], out_hbm.at[:, cut], o_sem.at[n])
+
+    for n in range(cuts):
         cut = slice(n * step, (n + 1) * step)
         total = jnp.zeros((BLOCK, step), F32)
         for d in range(NY):
@@ -598,53 +642,33 @@
             if o or p:
                 d_copy(o, p).start()
 
-    d_right(1).wait_recv()
-    d_left(1).wait_recv()
-    d_on_right().wait_recv()
-    d_on_left().wait_recv()
-    w_beside(1, wd).start()
-    w_beside(1, wd).wait_recv()
+    for d in range(NY):
+        d_beside(d).wait_recv()
     for group_at in ((0,), (3, 1), (2,)):
         for d in group_at:
             o = (NY - d) % NY
             for p in range(2):
                 if o or p:
                     d_copy(o, p).wait_recv()
-        for n in range(out_ref.shape[1] // step):
+        for n in range(cuts):
             cut = slice(n * step, (n + 1) * step)
             total = acc[:, cut]
             for d in group_at:
                 total = total + jnp.dot(in_d[d], wd[d, :, cut], preferred_element_type=F32)
             if group_at == (2,):
                 out_ref[:, cut] = total.astype(BF16)
+                out_copy(n).start()
             else:
                 acc[:, cut] = total
 
-    def drain(r, carry):
-        to_right(r).wait_send()
-        to_left(r).wait_send()
-        on_right(r).wait_send()
-        on_left(r).wait_send()
-        for o in range(NY):
-            beside(o, r).wait_send()
-        for k in range(1, NX):
-            w_third(r, k).wait_send()
-        return carry
-
-    lax.fori_loop(0, chunks, drain, 0)
-    for o in (1, 2, 3):
-        w_first(o).wait_send()
-    for j in range(1, NZ):
-        w_second(j).wait_send()
     for i in range(2):
         d_right(i).wait_send()
         d_left(i).wait_send()
     d_on_right().wait_send()
     d_on_left().wait_send()
-    w_beside(0, wc).wait_send()
-    w_beside(1, wd).wait_send()
-    for k in (1, 2, 3):
-        x_copy(k).wait_send()
+    w_beside().wait_send()
+    for d in range(NY):
+        d_beside(d).wait_send()
 
     @pl.when(place + 1 < sp)
     def _():
@@ -654,7 +678,8 @@
 
         @pl.when(z + i + 1 < NZ)
         def _(i=i):
-            z_copy(i).wait_send()
+            z_copy(i, 0).wait_send()
+            z_copy(i, 1).wait_send()
 
     @pl.when(z + 4 < NZ)
     def _():
@@ -664,6 +689,8 @@
         ln_copy(o, p).wait_send()
         c_copy(o, p).wait_send()
         d_copy(o, p).wait_send()
+    for n in range(cuts):
+        out_copy(n).wait()
 
 
 def local(
@@ -684,8 +711,9 @@
         layer_kernel,
         out_shape=jax.ShapeDtypeStruct((BLOCK, wide), BF16),
         in_specs=[hbm] * 17,
-        out_specs=pl.BlockSpec(memory_space=pltpu.VMEM),
+        out_specs=hbm,
         scratch_shapes=[
+            vm((BLOCK, wide), BF16),
             vm((rows, depth), BF16),
             vm((depth, 8 * width), BF16),
             vm((7, rows, width), BF16),
@@ -732,14 +760,15 @@
             dma((NY - 1,)), dma((NY - 1,)),
             dma((NZ - 1,)), dma((NZ - 1,)),
             dma((NZ, NX - 1)), dma((NZ, NX - 1)),
-            dma((2,)), dma((2,)),
+            dma((NY + 1,)), dma((NY + 1,)),
             dma((6,)), dma((6,)),
             dma((NX - 1,)), dma((NX - 1,)),
-            dma((3,)), dma((3,)),
+            dma((5,)), dma((5,)),
             dma((1,)), dma((1,)),
             dma((7,)), dma((7,)),
             dma((7,)), dma((7,)),
             dma((7,)), dma((7,)),
+            dma((4,)),
         ],
         compiler_params=pltpu.CompilerParams(
             collective_id=0, has_side_effects=True, vmem_limit_bytes=60 * 1024 * 1024

time: 79.7 us -> 70.1 us (0.88)
  Pallas kernels: 77.7 us -> 68.1 us
    pallas_call x1, Pallas kernels: 77.7 us -> 68.1 us  [local(): pl.pallas_call(layer_kernel, out_shape=jax.ShapeDtypeStruct((BLOCK, wide)...]
where the time goes in v2:
time: 70.1 us; the launch traced here: 70 us
  Pallas kernels  68.1 us (97%)
  local copies, waits for them, and re-layouts  1.88 us (3%)
    pallas_call x1, Pallas kernels, local(): pl.pallas_call(layer_kernel, out_shape=jax.ShapeDtypeStruct((BLOCK, wide)...  68.1 us
    unnamed x1, local copies, waits for them, and re-layouts  1.88 us

profile of v2, /device:TPU:1, one launch (start us, length us, event | category | flops | bytes accessed | tf_op | source)
XLA Modules:
  0.0 70.0 jit_solution(4814557504413923637)
XLA Ops:
  0.0 68.1 %layer.1 = bf16[128,2048]{1,0:T(8,128)(2,1)} custom-call(bf16[1024,256]{1,0:T(8,128)(2,1)} %tok_hbm.1, bf16[2048,128]{1,0:T(8,128)(2,1)} %wq_hbm.1, bf16[2048,128]{1,0:T(8,128)(2,1)} %wk_hbm.1, bf16[2048,128]{1,0:T(8,128)(2,1)} %wv_hbm.1, bf16[2048,128]{1,0:T(8,128)(2,1)} %wdg_hbm.1, bf16[2048,128]{1,0:T(8,128)(2,1)} %wgv_hbm.1, bf16[2048,128]{1,0:T(8,128)(2,1)} %wgg_hbm.1, ...), custom_call_target="tpu_custom_call" | custom-call | flops 10000000000 | bytes 20000000 | tf_op jit(solution)/shard_map/layer/pallas_call | solution.py:710
  68.1 1.9 %copy.19 = bf16[128,2048]{1,0:T(8,128)(2,1)} copy(bf16[128,2048]{1,0:T(8,128)(2,1)} %layer.1) | data formatting | bytes 1048576

commit v3 on v2

--- a/solution.py
+++ b/solution.py
@@ -42,10 +42,7 @@
     wd, wc, lhs_s, corr_s, score_s, wt_s, tail_s, state_ref, outa_s, outb_s,
     xin, zs, zr, zs4, zr4, padded, filtered, halo_out, halo_in, sums_out, sums_in,
     cm_s, dsend, in_d, in_c, acc, gate_s,
-    l_sem, r_send, r_recv, l_send, l_recv, fr_send, fr_recv, fl_send, fl_recv,
-    b_send, b_recv, w1_send, w1_recv, w2_send, w2_recv, w3_send, w3_recv, wb_send, wb_recv,
-    wd_send, wd_recv, x_send, x_recv, z_send, z_recv, h_send, h_recv, ln_send, ln_recv,
-    c_send, c_recv, d_send, d_recv, o_sem,
+    l_sem, sent, a_recv, f_recv, b_recv, w2_recv, got, z_send, z_recv,
 ):
     rows, part = tok_hbm.shape
     chunks = rows // BLOCK
@@ -91,15 +88,15 @@
 
     loads = {"tok": load(0, tok_hbm, full.at[:, columns(me)]), "oc": load(1, oc_hbm, wc.at[0, :BLOCK, :])}
     for i, src in enumerate((wq_hbm, wk_hbm, wv_hbm, wdg_hbm, wgv_hbm, wgg_hbm, wcg_hbm)):
-        loads[i] = load(2 + i, src, w_all.at[:, i * width : (i + 1) * width])
-    loads["wb"] = load(9, wb_hbm, wb_s)
-    loads["wdec"] = load(10, wdec_hbm, wdec_s)
-    loads["rate"] = load(11, rate_hbm, rate_s)
-    loads["gain"] = load(12, gain_hbm, gain_s)
-    loads["taps"] = load(13, taps_hbm, taps_s)
-    loads["lng"] = load(14, lng_hbm, lng_s)
-    loads["lns"] = load(15, lns_hbm, lns_s)
-    loads["od"] = load(16, od_hbm, wd.at[0, :BLOCK, :])
+        loads[i] = load(2, src, w_all.at[:, i * width : (i + 1) * width])
+    loads["wb"] = load(3, wb_hbm, wb_s)
+    loads["wdec"] = load(4, wdec_hbm, wdec_s)
+    loads["rate"] = load(5, rate_hbm, rate_s)
+    loads["gain"] = load(6, gain_hbm, gain_s)
+    loads["taps"] = load(7, taps_hbm, taps_s)
+    loads["lng"] = load(8, lng_hbm, lng_s)
+    loads["lns"] = load(9, lns_hbm, lns_s)
+    loads["od"] = load(10, od_hbm, wd.at[0, :BLOCK, :])
     for copy in loads.values():
         copy.start()
 
@@ -109,28 +106,34 @@
             device_id=device, device_id_type=MESH,
         )
 
+    def settle(ref, send):
+        remote(ref, ref, sent.at[send], got.at[0], tp=sibling).wait_send()
+
+    def landed(ref, recv):
+        remote(ref, ref, sent.at[0], recv, tp=sibling).wait_recv()
+
     def to_right(r):
         block = full.at[at(r), columns(me)]
-        return remote(block, block, r_send.at[r], r_recv.at[r], tp=tp_at(1))
+        return remote(block, block, sent.at[0], a_recv.at[r], tp=tp_at(1))
 
     def to_left(r):
         block = full.at[at(r), columns(me)]
-        return remote(block, block, l_send.at[r], l_recv.at[r], tp=tp_at(-1))
+        return remote(block, block, sent.at[1], a_recv.at[r], tp=tp_at(-1))
 
     def half(r, i):
         return pl.ds(pl.multiple_of(r * BLOCK + i * (BLOCK // 2), BLOCK // 2), BLOCK // 2)
 
     def on_right(r):
         block = full.at[half(r, 0), columns(tp_at(-1))]
-        return remote(block, block, fr_send.at[r], fr_recv.at[r], tp=tp_at(1))
+        return remote(block, block, sent.at[2], f_recv.at[r], tp=tp_at(1))
 
     def on_left(r):
         block = full.at[half(r, 1), columns(tp_at(1))]
-        return remote(block, block, fl_send.at[r], fl_recv.at[r], tp=tp_at(-1))
+        return remote(block, block, sent.at[3], f_recv.at[r], tp=tp_at(-1))
 
     def beside(o, r):
         block = full.at[at(r), columns(tp_at(o))]
-        return remote(block, block, b_send.at[o, r], b_recv.at[o, r], tp=sibling)
+        return remote(block, block, sent.at[4], b_recv.at[r], tp=sibling)
 
     zrows = BLOCK // NZ
     xcols = wc.shape[2] // NX
@@ -144,29 +147,29 @@
     def w_first(o):
         a, b = wpiece(0)
         return remote(
-            wc.at[0, a, b], wc.at[NY - o, a, b], w1_send.at[o - 1], w1_recv.at[o - 1], tp=tp_at(o)
+            wc.at[0, a, b], wc.at[NY - o, a, b], sent.at[5], got.at[1], tp=tp_at(o)
         )
 
     def w_second(j):
         a, b = wpiece(0)
         block = wc.at[pl.ds(1, NY - 1), a, b]
-        return remote(block, block, w2_send.at[j - 1], w2_recv.at[j - 1], sp=sp_at(j, 0))
+        return remote(block, block, sent.at[6], w2_recv.at[j - 1], sp=sp_at(j, 0))
 
     def w_third(i, k):
         a, b = wpiece(i)
         block = wc.at[pl.ds(1, NY - 1), a, b]
-        return remote(block, block, w3_send.at[i, k - 1], w3_recv.at[i, k - 1], sp=sp_at(0, k))
+        return remote(block, block, sent.at[7], got.at[2], sp=sp_at(0, k))
 
     def w_beside():
         return remote(
             wc.at[:, pl.ds(0, BLOCK), :], wc.at[:, pl.ds(BLOCK, BLOCK), :],
-            wb_send.at[NY], wb_recv.at[NY], tp=sibling,
+            sent.at[8], got.at[3], tp=sibling,
         )
 
     def d_beside(d):
         return remote(
             wd.at[d, pl.ds(0, BLOCK), :], wd.at[d, pl.ds(BLOCK, BLOCK), :],
-            wb_send.at[d], wb_recv.at[d], tp=sibling,
+            sent.at[9], got.at[4], tp=sibling,
         )
 
     hb = BLOCK // 2
@@ -174,25 +177,25 @@
     def d_right(i):
         return remote(
             wd.at[0, pl.ds(i * hb, hb), :], wd.at[3, pl.ds(i * hb, hb), :],
-            wd_send.at[i], wd_recv.at[i], tp=tp_at(1),
+            sent.at[10], got.at[5], tp=tp_at(1),
         )
 
     def d_left(i):
         return remote(
             wd.at[0, pl.ds((1 - i) * hb, hb), :], wd.at[1, pl.ds((1 - i) * hb, hb), :],
-            wd_send.at[2 + i], wd_recv.at[2 + i], tp=tp_at(-1),
+            sent.at[10], got.at[5], tp=tp_at(-1),
         )
 
     def d_on_right():
         return remote(
             wd.at[3, pl.ds(0, hb), :], wd.at[2, pl.ds(0, hb), :],
-            wd_send.at[4], wd_recv.at[4], tp=tp_at(1),
+            sent.at[11], got.at[6], tp=tp_at(1),
         )
 
     def d_on_left():
         return remote(
             wd.at[1, pl.ds(hb, hb), :], wd.at[2, pl.ds(hb, hb), :],
-            wd_send.at[5], wd_recv.at[5], tp=tp_at(-1),
+            sent.at[11], got.at[6], tp=tp_at(-1),
         )
 
     loads["tok"].wait()
@@ -226,14 +229,12 @@
     rate = jnp.exp(
         jnp.sum(jnp.where(lane8 == me, rate_s[...], 0.0), axis=1, keepdims=True)
     )
-    for i in range(7):
-        loads[i].wait()
+    load(2, w_all.at[:, : 7 * width], w_all.at[:, : 7 * width]).wait()
     loads["taps"].wait()
     tapf_s[:kernel, :] = taps_s[...].astype(F32)
 
     def arrive(r):
-        to_right(r).wait_recv()
-        to_left(r).wait_recv()
+        landed(full.at[at(r), pl.ds(0, 2 * part)], a_recv.at[r])
         on_right(r).start()
         on_left(r).start()
         beside(3, r).start()
@@ -245,8 +246,7 @@
             to_left(r + AHEAD).start()
 
     def arrive_far(r):
-        on_right(r).wait_recv()
-        on_left(r).wait_recv()
+        landed(full.at[at(r), pl.ds(0, part)], f_recv.at[r])
         beside(2, r).start()
 
     def w_pass(r):
@@ -254,11 +254,12 @@
         for k in (2, 1, 3):
             w_third(r, k).start()
 
-    def chunk(r):
-        for o in range(NY):
-            beside(o, r).wait_recv()
-        here = at(r)
-        squares = jnp.zeros((BLOCK, 1), F32)
+    def chunk(r, count=1):
+        for i in range(count):
+            landed(full.at[at(r + i), pl.ds(0, NY * part)], b_recv.at[r + i])
+        size = count * BLOCK
+        here = pl.ds(pl.multiple_of(r * BLOCK, BLOCK), size)
+        squares = jnp.zeros((size, 1), F32)
         for b in range(2 * NY):
             piece = full[here, b * part : (b + 1) * part].astype(F32)
             squares = squares + jnp.sum(piece * piece, axis=1, keepdims=True)
@@ -335,11 +336,15 @@
         while size < BLOCK:
             if size in pauses:
                 yield
-            level = (differ >= size) & (differ < 2 * size)
-            moved = [mm(jnp.where(level, ch[1], 0.0), ch[3]) for ch in chains]
-            for ch, part_ in zip(chains, moved):
-                ch[3] = ch[3] - mm(ch[3], part_)
-            size *= 2
+            level = (differ >= size) & (differ < 4 * size)
+            steps = [mm(ch[3], jnp.where(level, ch[1], 0.0)) for ch in chains]
+            once = [ch[3] - mm(step, ch[3]) for ch, step in zip(chains, steps)]
+            twice = [mm(step, step) for step in steps]
+            for ch, one, two in zip(chains, once, twice):
+                ch[3] = one + mm(two, one)
+            size *= 4
+        if size in pauses:
+            yield
         for c, lower, right, inverse in chains:
             solved = mm(inverse, right)
             corr_s[c * BLOCK : (c + 1) * BLOCK, :] = solved[:, :width]
@@ -347,8 +352,7 @@
         lax.fori_loop(first, first + count, advance, 0)
 
     state_ref[...] = ident
-    for o in (1, 2, 3):
-        w_first(o).wait_recv()
+    landed(wc.at[0, pl.ds(0, 3 * zrows), pl.ds(0, xcols)], got.at[1])
     for j in range(1, NZ):
         w_second(j).start()
     for k in (2, 1, 3):
@@ -366,25 +370,23 @@
         return carry
 
     lax.fori_loop(2, 6, steady, 0)
-    early = delta_group(0, 4, (8, 64))
+    early = delta_group(0, 4, (8, BLOCK))
     arrive(6)
     arrive_far(5)
     next(early)
-    chunk(4)
     w_pass(6)
     arrive(7)
+    arrive_far(6)
+    next(early)
+    chunk(4, 2)
+    w_pass(7)
+    arrive_far(7)
     loads["od"].wait()
     for i in range(2):
         d_right(i).start()
         d_left(i).start()
-    arrive_far(6)
-    next(early)
-    chunk(5)
-    w_pass(7)
-    arrive_far(7)
     list(early)
-    chunk(6)
-    chunk(7)
+    chunk(6, 2)
 
     def unit(t):
         value = proj[4, at(t), :].astype(F32)
@@ -395,7 +397,7 @@
     units = unit(chunks - 1)
     halo_out[...] = units[BLOCK - halo :, :]
     halo_copy = remote(
-        halo_out, halo_in, h_send.at[0], h_recv.at[0], sp=lax.rem(place + 1, sp)
+        halo_out, halo_in, sent.at[13], got.at[8], sp=lax.rem(place + 1, sp)
     )
 
     @pl.when(place + 1 < sp)
@@ -407,7 +409,7 @@
     xin[0] = state_ref[...].astype(BF16)
 
     def x_copy(k):
-        return remote(xin.at[0], xin.at[k], x_send.at[k - 1], x_recv.at[k - 1], sp=sp_at(0, k))
+        return remote(xin.at[0], xin.at[k], sent.at[12], got.at[7], sp=sp_at(0, k))
 
     for k in (2, 1, 3):
         x_copy(k).start()
@@ -416,9 +418,7 @@
         unit(t)
         return carry
 
-    for i in range(NZ):
-        for k in range(1, NX):
-            w_third(i, k).wait_recv()
+    landed(wc.at[pl.ds(1, NY - 1), pl.ds(0, 96), :], got.at[2])
     w_beside().start()
     lax.fori_loop(0, chunks - 1, unit_loop, 0)
 
@@ -436,16 +436,32 @@
         return carry
 
     lax.fori_loop(1, chunks, conv, 0)
-    for i in range(2):
-        d_right(i).wait_recv()
-        d_left(i).wait_recv()
+
+    @pl.when(place >= 1)
+    def _():
+        halo_copy.wait_recv()
+
+    @pl.when(place < 1)
+    def _():
+        halo_in[...] = jnp.zeros(halo_in.shape, BF16)
+
+    padded[:halo, :] = halo_in[...].astype(F32)
+    conv(0, 0)
+
+    def ln_copy(o, p):
+        i = 2 * o + p - 1
+        return remote(sums_out, sums_in.at[i], sent.at[14], got.at[9], tp=tp_at(o, p))
+
+    others = [(2, 0), (2, 1), (1, 0), (1, 1), (3, 0), (3, 1), (0, 1)]
+    for o, p in others:
+        ln_copy(o, p).start()
+    landed(wd.at[pl.ds(0, 2), pl.ds(0, BLOCK), :], got.at[5])
     d_on_right().start()
     d_on_left().start()
     for d in (0, 1, 3):
         d_beside(d).start()
 
-    for k in (1, 2, 3):
-        x_copy(k).wait_recv()
+    landed(xin.at[pl.ds(1, NX - 1)], got.at[7])
 
     def piece(i):
         return xin[lax.rem(x - i + NX, NX)]
@@ -492,44 +508,15 @@
     def _():
         zr4[...] = jnp.zeros(zr4.shape, BF16)
 
-    @pl.when(place >= 1)
-    def _():
-        halo_copy.wait_recv()
-
-    @pl.when(place < 1)
-    def _():
-        halo_in[...] = jnp.zeros(halo_in.shape, BF16)
-
-    padded[:halo, :] = halo_in[...].astype(F32)
-    conv(0, 0)
-
-    def ln_copy(o, p):
-        i = 2 * o + p - 1
-        return remote(
-            sums_out, sums_in.at[i], ln_send.at[i], ln_recv.at[i], tp=tp_at(o, p)
-        )
-
-    others = [(2, 0), (2, 1), (1, 0), (1, 1), (3, 0), (3, 1), (0, 1)]
-    for o, p in others:
-        ln_copy(o, p).start()
-    def drain(r, carry):
-        to_right(r).wait_send()
-        to_left(r).wait_send()
-        on_right(r).wait_send()
-        on_left(r).wait_send()
-        for o in range(NY):
-            beside(o, r).wait_send()
-        for k in range(1, NX):
-            w_third(r, k).wait_send()
-        return carry
-
-    lax.fori_loop(0, chunks, drain, 0)
-    for o in (1, 2, 3):
-        w_first(o).wait_send()
-    for j in range(1, NZ):
-        w_second(j).wait_send()
-    for k in (1, 2, 3):
-        x_copy(k).wait_send()
+    settle(full.at[:, columns(me)], 0)
+    settle(full.at[:, columns(me)], 1)
+    settle(full.at[pl.ds(0, rows // 2), columns(me)], 2)
+    settle(full.at[pl.ds(0, rows // 2), columns(me)], 3)
+    settle(full.at[:, pl.ds(0, NY * part)], 4)
+    settle(wc.at[0, pl.ds(0, 3 * zrows), pl.ds(0, xcols)], 5)
+    settle(wc.at[pl.ds(1, NY - 1), pl.ds(0, 7 * zrows), pl.ds(0, xcols)], 6)
+    settle(wc.at[pl.ds(1, NY - 1), pl.ds(0, 96), :], 7)
+    settle(xin.at[pl.ds(1, NX - 1)], 12)
 
     def left(i):
         return zs[i][:, :width]
@@ -544,8 +531,7 @@
     zs[1, :, :width] = mm(left(0), e1[:, :width]).astype(BF16)
     z_start(1, 0)
 
-    for o, p in others:
-        ln_copy(o, p).wait_recv()
+    landed(sums_in, got.at[9])
     loads["lng"].wait()
     loads["lns"].wait()
     loads["gain"].wait()
@@ -569,14 +555,13 @@
         return remote(
             cm_s.at[at(tp_at(o, p)), :],
             in_c.at[(NY - o) % NY, :, pl.ds(p * width, width)],
-            c_send.at[i], c_recv.at[i], tp=tp_at(o, p),
+            sent.at[15], got.at[10], tp=tp_at(o, p),
         )
 
     for o, p in others:
         c_copy(o, p).start()
     in_c[0, :, :width] = cm_s[at(me), :]
-    d_on_right().wait_recv()
-    d_on_left().wait_recv()
+    landed(wd.at[0, pl.ds(0, BLOCK), :], got.at[6])
     d_beside(2).start()
     z_wait(1, 1)
     zs4[...] = (mm(left(1), zr[1, :, width:]) + zs[1, :, width:].astype(F32)).astype(BF16)
@@ -594,14 +579,13 @@
         gate_s[here, :] = gain_s[...] * jax.nn.silu(proj[3, here, :].astype(F32))
 
     w_beside().wait_recv()
-    for o, p in others:
-        c_copy(o, p).wait_recv()
+    landed(dsend, got.at[10])
     step = 512
     cuts = out_ref.shape[1] // step
 
     def out_copy(n):
         cut = pl.ds(n * step, step)
-        return pltpu.make_async_copy(out_ref.at[:, cut], out_hbm.at[:, cut], o_sem.at[n])
+        return pltpu.make_async_copy(out_ref.at[:, cut], out_hbm.at[:, cut], l_sem.at[0])
 
     for n in range(cuts):
         cut = slice(n * step, (n + 1) * step)
@@ -620,7 +604,7 @@
         i = 2 * o + p - 1
         return remote(
             dsend.at[i], in_d.at[(NY - o) % NY, :, pl.ds(p * width, width)],
-            d_send.at[i], d_recv.at[i], tp=tp_at(o, p),
+            sent.at[16], got.at[0 if o == 0 else 11 if o == 2 else 12], tp=tp_at(o, p),
         )
 
     for batch in (others[:2], others[2:6], [(0, 1), (0, 0)]):
@@ -642,14 +626,9 @@
             if o or p:
                 d_copy(o, p).start()
 
-    for d in range(NY):
-        d_beside(d).wait_recv()
-    for group_at in ((0,), (3, 1), (2,)):
-        for d in group_at:
-            o = (NY - d) % NY
-            for p in range(2):
-                if o or p:
-                    d_copy(o, p).wait_recv()
+    landed(wd.at[:, pl.ds(0, BLOCK), :], got.at[4])
+    for group_at, count, sem in (((0,), 1, 0), ((3, 1), 4, 12), ((2,), 2, 11)):
+        landed(dsend.at[pl.ds(0, count)], got.at[sem])
         for n in range(cuts):
             cut = slice(n * step, (n + 1) * step)
             total = acc[:, cut]
@@ -661,14 +640,10 @@
             else:
                 acc[:, cut] = total
 
-    for i in range(2):
-        d_right(i).wait_send()
-        d_left(i).wait_send()
-    d_on_right().wait_send()
-    d_on_left().wait_send()
-    w_beside().wait_send()
-    for d in range(NY):
-        d_beside(d).wait_send()
+    settle(wc.at[:, pl.ds(0, BLOCK), :], 8)
+    settle(wd.at[:, pl.ds(0, BLOCK), :], 9)
+    settle(wd.at[pl.ds(0, 2), pl.ds(0, BLOCK), :], 10)
+    settle(wd.at[0, pl.ds(0, BLOCK), :], 11)
 
     @pl.when(place + 1 < sp)
     def _():
@@ -685,12 +660,10 @@
     def _():
         last_copy.wait_send()
 
-    for o, p in others:
-        ln_copy(o, p).wait_send()
-        c_copy(o, p).wait_send()
-        d_copy(o, p).wait_send()
-    for n in range(cuts):
-        out_copy(n).wait()
+    settle(sums_in, 14)
+    settle(dsend, 15)
+    settle(dsend, 16)
+    pltpu.make_async_copy(out_ref, out_hbm, l_sem.at[0]).wait()
 
 
 def local(
@@ -753,22 +726,15 @@
             vm((NY, BLOCK, 2 * width), BF16),
             vm((BLOCK, wide), F32),
             vm((rows, width), F32),
+            dma((11,)),
             dma((17,)),
-            dma((chunks,)), dma((chunks,)), dma((chunks,)), dma((chunks,)),
-            dma((chunks,)), dma((chunks,)), dma((chunks,)), dma((chunks,)),
-            dma((NY, chunks)), dma((NY, chunks)),
-            dma((NY - 1,)), dma((NY - 1,)),
-            dma((NZ - 1,)), dma((NZ - 1,)),
-            dma((NZ, NX - 1)), dma((NZ, NX - 1)),
-            dma((NY + 1,)), dma((NY + 1,)),
-            dma((6,)), dma((6,)),
-            dma((NX - 1,)), dma((NX - 1,)),
-            dma((5,)), dma((5,)),
-            dma((1,)), dma((1,)),
-            dma((7,)), dma((7,)),
-            dma((7,)), dma((7,)),
-            dma((7,)), dma((7,)),
-            dma((4,)),
+            dma((chunks,)),
+            dma((chunks,)),
+            dma((chunks,)),
+            dma((NZ - 1,)),
+            dma((13,)),
+            dma((5,)),
+            dma((5,)),
         ],
         compiler_params=pltpu.CompilerParams(
             collective_id=0, has_side_effects=True, vmem_limit_bytes=60 * 1024 * 1024

time: 70.1 us -> 65.1 us (0.929)
  Pallas kernels: 68.1 us -> 63.1 us
    pallas_call x1, Pallas kernels: 68.1 us -> 63.1 us  [local(): pl.pallas_call(layer_kernel, out_shape=jax.ShapeDtypeStruct((BLOCK, wide)...]
where the time goes in v3:
time: 65.1 us; the launch traced here: 65 us
  Pallas kernels  63.1 us (97%)
  local copies, waits for them, and re-layouts  1.88 us (3%)
    pallas_call x1, Pallas kernels, local(): pl.pallas_call(layer_kernel, out_shape=jax.ShapeDtypeStruct((BLOCK, wide)...  63.1 us
    unnamed x1, local copies, waits for them, and re-layouts  1.88 us

profile of v3, /device:TPU:1, one launch (start us, length us, event | category | flops | bytes accessed | tf_op | source)
XLA Modules:
  0.0 65.0 jit_solution(3042105889017575408)
XLA Ops:
  0.0 63.1 %layer.1 = bf16[128,2048]{1,0:T(8,128)(2,1)} custom-call(bf16[1024,256]{1,0:T(8,128)(2,1)} %tok_hbm.1, bf16[2048,128]{1,0:T(8,128)(2,1)} %wq_hbm.1, bf16[2048,128]{1,0:T(8,128)(2,1)} %wk_hbm.1, bf16[2048,128]{1,0:T(8,128)(2,1)} %wv_hbm.1, bf16[2048,128]{1,0:T(8,128)(2,1)} %wdg_hbm.1, bf16[2048,128]{1,0:T(8,128)(2,1)} %wgv_hbm.1, bf16[2048,128]{1,0:T(8,128)(2,1)} %wgg_hbm.1, ...), custom_call_target="tpu_custom_call" | custom-call | flops 10000000000 | bytes 20000000 | tf_op jit(solution)/shard_map/layer/pallas_call | solution.py:683
  63.1 1.9 %copy.19 = bf16[128,2048]{1,0:T(8,128)(2,1)} copy(bf16[128,2048]{1,0:T(8,128)(2,1)} %layer.1) | data formatting | bytes 1048576

commit v4 on v3

--- a/solution.py
+++ b/solution.py
@@ -6,7 +6,8 @@
 from jax.sharding import PartitionSpec as P
 
 BLOCK = 128
-AHEAD = 3
+AHEAD = 4
+LAG = 2
 TINY_NORM = 1e-06
 TINY_VAR = 1e-05
 HIGHEST = lax.Precision.HIGHEST
@@ -240,8 +241,7 @@
         beside(3, r).start()
         beside(1, r).start()
 
-        @pl.when(r + AHEAD < chunks)
-        def _():
+        if r + AHEAD < chunks:
             to_right(r + AHEAD).start()
             to_left(r + AHEAD).start()
 
@@ -254,7 +254,7 @@
         for k in (2, 1, 3):
             w_third(r, k).start()
 
-    def chunk(r, count=1):
+    def chunk_steps(r, count):
         for i in range(count):
             landed(full.at[at(r + i), pl.ds(0, NY * part)], b_recv.at[r + i])
         size = count * BLOCK
@@ -264,6 +264,7 @@
             piece = full[here, b * part : (b + 1) * part].astype(F32)
             squares = squares + jnp.sum(piece * piece, axis=1, keepdims=True)
         inv_rms = lax.rsqrt(squares / (part * 2 * NY) + TINY_NORM)
+        yield
         for j in range(4):
             summed = jnp.dot(
                 full[here, :], w_all[:, j * 256 : (j + 1) * 256], preferred_element_type=F32
@@ -279,6 +280,14 @@
                 gates_ref[here, :] = jnp.where(
                     lane == 0, jax.nn.sigmoid(raw), jnp.where(lane == 1, -rate * softplus, 0.0)
                 )
+            yield
+
+    def chunk(r, count):
+        list(chunk_steps(r, count))
+
+    def take(steps, count):
+        for _ in range(count):
+            next(steps)
 
     row_id = lax.broadcasted_iota(jnp.int32, (BLOCK, BLOCK), 0)
     col_id = lax.broadcasted_iota(jnp.int32, (BLOCK, BLOCK), 1)
@@ -330,26 +339,26 @@
         outb_s[at(c), :] = out[:, width:]
         return carry
 
-    def delta_group(first, count, pauses=()):
+    def delta_group(first, count, until):
         chains = [prepare(first + i) for i in range(count)]
+        yield
         size = 2
         while size < BLOCK:
-            if size in pauses:
-                yield
             level = (differ >= size) & (differ < 4 * size)
             steps = [mm(ch[3], jnp.where(level, ch[1], 0.0)) for ch in chains]
+            yield
             once = [ch[3] - mm(step, ch[3]) for ch, step in zip(chains, steps)]
             twice = [mm(step, step) for step in steps]
+            yield
             for ch, one, two in zip(chains, once, twice):
                 ch[3] = one + mm(two, one)
             size *= 4
-        if size in pauses:
             yield
         for c, lower, right, inverse in chains:
             solved = mm(inverse, right)
             corr_s[c * BLOCK : (c + 1) * BLOCK, :] = solved[:, :width]
             lhs_s[c, :BLOCK, :] = solved[:, width:].astype(BF16)
-        lax.fori_loop(first, first + count, advance, 0)
+        lax.fori_loop(first, until, advance, 0)
 
     state_ref[...] = ident
     landed(wc.at[0, pl.ds(0, 3 * zrows), pl.ds(0, xcols)], got.at[1])
@@ -357,34 +366,32 @@
         w_second(j).start()
     for k in (2, 1, 3):
         w_third(0, k).start()
-    arrive(0)
-    arrive(1)
-    arrive_far(0)
-    w_pass(1)
-
-    def steady(r, carry):
-        arrive(r)
-        arrive_far(r - 1)
-        chunk(r - 2)
-        w_pass(r)
-        return carry
-
-    lax.fori_loop(2, 6, steady, 0)
-    early = delta_group(0, 4, (8, BLOCK))
-    arrive(6)
-    arrive_far(5)
-    next(early)
-    w_pass(6)
-    arrive(7)
-    arrive_far(6)
-    next(early)
-    chunk(4, 2)
-    w_pass(7)
-    arrive_far(7)
-    loads["od"].wait()
-    for i in range(2):
-        d_right(i).start()
-        d_left(i).start()
+    early = delta_group(0, 4, 2)
+    for t in range(chunks + LAG):
+        if t < chunks:
+            arrive(t)
+        if t == chunks - 1:
+            loads["od"].wait()
+            for i in range(2):
+                d_right(i).start()
+                d_left(i).start()
+        if 1 <= t < NZ:
+            w_pass(t)
+        k = t - LAG
+        if k < 0:
+            continue
+        arrive_far(k)
+        if k == 2 or k == 4:
+            chunk(k - 2, 2)
+        if k == 5:
+            take(early, 4)
+        if k == 6:
+            woven = chunk_steps(4, 2)
+            for _ in range(5):
+                next(woven)
+                next(early)
+            list(woven)
+            next(early)
     list(early)
     chunk(6, 2)
 
@@ -404,7 +411,12 @@
     def _():
         halo_copy.start()
 
-    list(delta_group(4, 4))
+    late = delta_group(4, 4, 8)
+    take(late, 2)
+    advance(2, 0)
+    take(late, 3)
+    advance(3, 0)
+    list(late)
 
     xin[0] = state_ref[...].astype(BF16)
 
@@ -561,8 +573,6 @@
     for o, p in others:
         c_copy(o, p).start()
     in_c[0, :, :width] = cm_s[at(me), :]
-    landed(wd.at[0, pl.ds(0, BLOCK), :], got.at[6])
-    d_beside(2).start()
     z_wait(1, 1)
     zs4[...] = (mm(left(1), zr[1, :, width:]) + zs[1, :, width:].astype(F32)).astype(BF16)
 
@@ -570,6 +580,8 @@
     def _():
         last_copy.start()
 
+    landed(wd.at[0, pl.ds(0, BLOCK), :], got.at[6])
+    d_beside(2).start()
     z_wait(1, 0)
     e3 = compose(e1, zr[1])
     reach = compose(inner, e3)

time: 65.1 us -> 62.7 us (0.963)
  Pallas kernels: 63.1 us -> 60.7 us
    pallas_call x1, Pallas kernels: 63.1 us -> 60.7 us  [local(): pl.pallas_call(layer_kernel, out_shape=jax.ShapeDtypeStruct((BLOCK, wide)...]
where the time goes in v4:
time: 62.7 us; the launch traced here: 62.6 us
  Pallas kernels  60.7 us (97%)
  local copies, waits for them, and re-layouts  1.88 us (3%)
    pallas_call x1, Pallas kernels, local(): pl.pallas_call(layer_kernel, out_shape=jax.ShapeDtypeStruct((BLOCK, wide)...  60.7 us
    unnamed x1, local copies, waits for them, and re-layouts  1.88 us

profile of v4, /device:TPU:1, one launch (start us, length us, event | category | flops | bytes accessed | tf_op | source)
XLA Modules:
  0.0 62.6 jit_solution(15268657271746292880)
XLA Ops:
  0.0 60.7 %layer.1 = bf16[128,2048]{1,0:T(8,128)(2,1)} custom-call(bf16[1024,256]{1,0:T(8,128)(2,1)} %tok_hbm.1, bf16[2048,128]{1,0:T(8,128)(2,1)} %wq_hbm.1, bf16[2048,128]{1,0:T(8,128)(2,1)} %wk_hbm.1, bf16[2048,128]{1,0:T(8,128)(2,1)} %wv_hbm.1, bf16[2048,128]{1,0:T(8,128)(2,1)} %wdg_hbm.1, bf16[2048,128]{1,0:T(8,128)(2,1)} %wgv_hbm.1, bf16[2048,128]{1,0:T(8,128)(2,1)} %wgg_hbm.1, ...), custom_call_target="tpu_custom_call" | custom-call | flops 10000000000 | bytes 20000000 | tf_op jit(solution)/shard_map/layer/pallas_call | solution.py:695
  60.7 1.9 %copy.19 = bf16[128,2048]{1,0:T(8,128)(2,1)} copy(bf16[128,2048]{1,0:T(8,128)(2,1)} %layer.1) | data formatting | bytes 1048576

commit v5 on v4

--- a/solution.py
+++ b/solution.py
@@ -7,7 +7,7 @@
 
 BLOCK = 128
 AHEAD = 4
-LAG = 2
+LAG = 3
 TINY_NORM = 1e-06
 TINY_VAR = 1e-05
 HIGHEST = lax.Precision.HIGHEST
@@ -619,7 +619,7 @@
             sent.at[16], got.at[0 if o == 0 else 11 if o == 2 else 12], tp=tp_at(o, p),
         )
 
-    for batch in (others[:2], others[2:6], [(0, 1), (0, 0)]):
+    for batch in (others[:6], [(0, 1), (0, 0)]):
         places = [at(tp_at(o, p)) for o, p in batch]
         results = [outb_s[pos, :] + mm(outa_s[pos, :], carried) for pos in places]
         scales = [

time: 62.7 us -> 62.2 us (level); the launches traced: 62.6 us -> 61.4 us
  Pallas kernels: 60.7 us -> 59.5 us
    pallas_call x1, Pallas kernels: 60.7 us -> 59.5 us  [local(): pl.pallas_call(layer_kernel, out_shape=jax.ShapeDtypeStruct((BLOCK, wide)...]
where the time goes in v5:
time: 62.2 us; the launch traced here: 61.4 us
  Pallas kernels  59.5 us (96%)
  local copies, waits for them, and re-layouts  1.88 us (3%)
    pallas_call x1, Pallas kernels, local(): pl.pallas_call(layer_kernel, out_shape=jax.ShapeDtypeStruct((BLOCK, wide)...  59.5 us
    unnamed x1, local copies, waits for them, and re-layouts  1.88 us

profile of v5, /device:TPU:1, one launch (start us, length us, event | category | flops | bytes accessed | tf_op | source)
XLA Modules:
  0.0 61.4 jit_solution(18035243399155517219)
XLA Ops:
  0.0 59.5 %layer.1 = bf16[128,2048]{1,0:T(8,128)(2,1)} custom-call(bf16[1024,256]{1,0:T(8,128)(2,1)} %tok_hbm.1, bf16[2048,128]{1,0:T(8,128)(2,1)} %wq_hbm.1, bf16[2048,128]{1,0:T(8,128)(2,1)} %wk_hbm.1, bf16[2048,128]{1,0:T(8,128)(2,1)} %wv_hbm.1, bf16[2048,128]{1,0:T(8,128)(2,1)} %wdg_hbm.1, bf16[2048,128]{1,0:T(8,128)(2,1)} %wgv_hbm.1, bf16[2048,128]{1,0:T(8,128)(2,1)} %wgg_hbm.1, ...), custom_call_target="tpu_custom_call" | custom-call | flops 10000000000 | bytes 20000000 | tf_op jit(solution)/shard_map/layer/pallas_call | solution.py:695
  59.5 1.9 %copy.19 = bf16[128,2048]{1,0:T(8,128)(2,1)} copy(bf16[128,2048]{1,0:T(8,128)(2,1)} %layer.1) | data formatting | bytes 1048576
